TPU v7x, 32 devices: a whole 2x2x4 slice. The times are simulated.
32 devices in a mesh: rep: 4 (over z), fs: 4 (over y, x), tp: 2 (over core).
Axes of the slice: x: 2, y: 2, z: 4, core: 2. Of those that a mesh axis runs over, the one named last changes fastest.
Arguments:
- hidden_in: bfloat16 [2048, 2048], P('rep'), may hold values from -6 to 6
- cotangent: bfloat16 [2048, 2048], P('rep'), may hold values from -3 to 3
- w_up: bfloat16 [2048, 8192], P('rep', ('fs', 'tp')), may hold values from -0.125 to 0.125
- w_down: bfloat16 [8192, 2048], P(('fs', 'tp'), 'rep'), may hold values from -0.0625 to 0.0625
Outputs:
- input_grad: bfloat16 [2048, 2048], P('rep')
- up_grad: float32 [2048, 8192], P('rep', ('fs', 'tp'))
- down_grad: float32 [8192, 2048], P(('fs', 'tp'), 'rep')
All inputs are finite; a program needn't handle non-finite values.
Results may differ from a plain program's by a relative error of at most 0.017.
Values may be sent and summed in bfloat16 or wider, within the bound.
No kernel may reach another device: no remote copies, remote signals or barrier semaphores. Data moves between devices by JAX's collectives and lax.ppermute only.
A program may use at most 64 MiB of HBM per device.

v0:
```python
import jax
import jax.numpy as jnp
from jax import lax
from jax.sharding import PartitionSpec as P


def contract_last(left, right):
    return lax.dot_general(
        left, right, (((1,), (1,)), ((), ())), preferred_element_type=jnp.float32
    )


def contract_first(left, right):
    return lax.dot_general(
        left, right, (((0,), (0,)), ((), ())), preferred_element_type=jnp.float32
    )


def on_device(hidden_in, cotangent, w_up, w_down):
    up_full = lax.all_gather(w_up, "rep", axis=0, tiled=True)
    back_grad = contract_last(cotangent, lax.all_gather(w_down, "rep", axis=1, tiled=True))
    preact = jnp.dot(hidden_in, up_full, preferred_element_type=jnp.float32)
    active = jnp.maximum(preact, 0.0)
    hidden = (active * active).astype(jnp.bfloat16)
    slopes = (2.0 * active * back_grad).astype(jnp.bfloat16)
    grad_upper = lax.psum_scatter(
        contract_first(hidden_in, slopes).astype(jnp.bfloat16),
        "rep",
        scatter_dimension=0,
        tiled=True,
    ).astype(jnp.float32)
    lower_rows = lax.psum_scatter(
        contract_first(cotangent, hidden).astype(jnp.bfloat16),
        "rep",
        scatter_dimension=0,
        tiled=True,
    ).astype(jnp.float32)
    down_grad = lower_rows.T
    partial_sum = contract_last(slopes, up_full).astype(jnp.bfloat16)
    input_grad = lax.psum(partial_sum, ("fs", "tp")).astype(jnp.float32).astype(jnp.bfloat16)
    return (input_grad, grad_upper, down_grad)


def solution(mesh):
    return jax.shard_map(
        on_device,
        mesh=mesh,
        in_specs=(P("rep", None), P("rep", None), P("rep", ("fs", "tp")), P(("fs", "tp"), "rep")),
        out_specs=(P("rep", None), P("rep", ("fs", "tp")), P(("fs", "tp"), "rep")),
        check_vma=False,
    )
```

profile of v0, /device:TPU:0, one launch (start us, length us, event | category | flops | bytes accessed | tf_op | source)
XLA Modules:
  0.0 414.7 jit_solution(14841434194789787365)
XLA Ops:
  7.2 0.0 copy-start
  7.2 0.0 all-gather.3.cloned.1.call-start
  7.2 0.7 all-gather.3.cloned.1.call-update
  7.9 0.0 all-gather.5.cloned.1.call-start
  8.0 0.7 all-gather.5.cloned.1.call-update
  8.7 0.0 reduce-scatter.3.cloned.1.call-start
  8.7 84.3 %all-gather.3.cloned.1.call-done = bf16[2048,1024]{1,0:T(8,128)(2,1)} async-done(((bf16[512,1024]{1,0:T(8,128)(2,1)}), bf16[2048,1024]{1,0:T(8,128)(2,1)}) %all-gather.3.cloned.1.call-update) | async-done | bytes 4194320 | tf_op jit(solution)/shard_map/all_gather | solution.py:20
  93.1 5.8 %fusion.2 = f32[512,1024]{1,0:T(8,128)} fusion(bf16[512,2048]{1,0:T(8,128)(2,1)S(1)} %copy-done, bf16[2048,1024]{1,0:T(8,128)(2,1)} %all-gather.3.cloned.1.call-done), kind=kOutput, calls=%fused_computation.8 | convolution fusion | flops 2147483648 | bytes 8388608 | tf_op jit(solution)/shard_map/dot_general | solution.py:22
  98.9 75.0 %all-gather.5.cloned.1.call-done = bf16[1024,2048]{1,0:T(8,128)(2,1)} async-done(((bf16[1024,512]{1,0:T(8,128)(2,1)}), bf16[1024,2048]{1,0:T(8,128)(2,1)}) %all-gather.5.cloned.1.call-update) | async-done | bytes 4194320 | tf_op jit(solution)/shard_map/all_gather | solution.py:21
  173.9 5.8 %multiply_convert_fusion.1 = bf16[512,1024]{1,0:T(8,128)(2,1)S(1)} fusion(f32[512,1024]{1,0:T(8,128)} %fusion.2, bf16[512,2048]{1,0:T(8,128)(2,1)} %param.5, bf16[1024,2048]{1,0:T(8,128)(2,1)} %all-gather.5.cloned.1.call-done), kind=kOutput, calls=%fused_computation.5 | convolution fusion | flops 2149580800 | bytes 9437184 | tf_op jit(solution)/shard_map/dot_general | solution.py:8
  179.7 4.4 %convert_bitcast_fusion.1 = bf16[2048,1024]{0,1:T(8,128)(2,1)} fusion(bf16[512,1024]{1,0:T(8,128)(2,1)S(1)} %multiply_convert_fusion.1, bf16[512,2048]{1,0:T(8,128)(2,1)S(1)} %copy-done), kind=kOutput, calls=%fused_computation.1 | convolution fusion | flops 2149580800 | bytes 7340032 | tf_op jit(solution)/shard_map/dot_general | solution.py:14
  184.1 0.0 reduce-scatter.3.cloned.1.call-update
  184.1 0.0 reduce-scatter.5.cloned.1.call-start
  184.2 6.6 %convert_bitcast_fusion = bf16[2048,1024]{0,1:T(8,128)(2,1)} fusion(bf16[512,2048]{1,0:T(8,128)(2,1)} %param.5, f32[512,1024]{1,0:T(8,128)} %fusion.2), kind=kOutput, calls=%fused_computation | convolution fusion | flops 2151153664 | bytes 8388608 | tf_op jit(solution)/shard_map/dot_general | solution.py:14
  190.8 0.0 reduce-scatter.5.cloned.1.call-update
  190.8 0.0 all-reduce.2.cloned.1.call-start
  190.8 5.9 %convolution_convert_fusion = bf16[512,2048]{1,0:T(8,128)(2,1)} fusion(bf16[512,1024]{1,0:T(8,128)(2,1)S(1)} %multiply_convert_fusion.1, bf16[2048,1024]{1,0:T(8,128)(2,1)} %all-gather.3.cloned.1.call-done), kind=kOutput, calls=%fused_computation.2 | convolution fusion | flops 2148532224 | bytes 7340032 | tf_op jit(solution)/shard_map/dot_general | solution.py:8
  196.7 0.0 all-reduce.2.cloned.1.call-update
  196.7 62.8 %reduce-scatter.3.cloned.1.call-done = bf16[512,1024]{0,1:T(8,128)(2,1)} async-done(((bf16[2048,1024]{0,1:T(8,128)(2,1)}), bf16[512,1024]{0,1:T(8,128)(2,1)}) %reduce-scatter.3.cloned.1.call-update) | async-done | bytes 1048592 | tf_op jit(solution)/shard_map/reduce_scatter | solution.py:26
  259.6 2.6 copy.7
  262.1 76.9 %reduce-scatter.5.cloned.1.call-done = bf16[512,1024]{0,1:T(8,128)(2,1)} async-done(((bf16[2048,1024]{0,1:T(8,128)(2,1)}), bf16[512,1024]{0,1:T(8,128)(2,1)}) %reduce-scatter.5.cloned.1.call-update) | async-done | bytes 1048592 | tf_op jit(solution)/shard_map/reduce_scatter | solution.py:32
  339.1 2.8 convert_bitcast_fusion.2
  341.9 63.1 %all-reduce.2.cloned.1.call-done = bf16[512,2048]{1,0:T(8,128)(2,1)} async-done(((bf16[512,2048]{1,0:T(8,128)(2,1)}), bf16[512,2048]{1,0:T(8,128)(2,1)}) %all-reduce.2.cloned.1.call-update) | async-done | bytes 2097168 | tf_op jit(solution)/shard_map/psum | solution.py:40
  405.0 3.2 copy.9
  (1 shorter events, 0.0 us)
Async XLA Ops:
  7.2 85.9 %copy-start = (bf16[512,2048]{1,0:T(8,128)(2,1)S(1)}, bf16[512,2048]{1,0:T(8,128)(2,1)}, u32[]{:S(2)}) copy-start(bf16[512,2048]{1,0:T(8,128)(2,1)} %param.4) | copy-start | bytes 6291460
  7.2 85.9 %all-gather.3.cloned.1.call-start = ((), (), s32[]{:S(2)}) async-start(), calls=%async_computation.2 | async-start | bytes 5242880 | tf_op jit(solution)/shard_map/all_gather | solution.py:20
  7.9 166.0 %all-gather.5.cloned.1.call-start = ((), (), s32[]{:S(2)}) async-start(), calls=%async_computation.3 | async-start | bytes 5242880 | tf_op jit(solution)/shard_map/all_gather | solution.py:21
  8.7 250.9 %reduce-scatter.3.cloned.1.call-start = ((), (), s32[]{:S(2)}) async-start(), calls=%async_computation.5 | async-start | bytes 5242880 | tf_op jit(solution)/shard_map/reduce_scatter | solution.py:26
  184.1 154.9 %reduce-scatter.5.cloned.1.call-start = ((), (), s32[]{:S(2)}) async-start(), calls=%async_computation.6 | async-start | bytes 5242880 | tf_op jit(solution)/shard_map/reduce_scatter | solution.py:32
  190.8 214.2 %all-reduce.2.cloned.1.call-start = ((), (), s32[]{:S(2)}) async-start(), calls=%async_computation.4 | async-start | bytes 4194304 | tf_op jit(solution)/shard_map/psum | solution.py:40
Sparse Core Ops, SparseCore 0:
  9.6 83.4 all-gather.2
  94.6 79.2 all-gather.4
  184.3 75.2 reduce-scatter.2
  261.7 77.2 reduce-scatter.4
  342.7 62.2 all-reduce.1
where the time goes:
time: 415 us
  waiting for transfers between devices  364 us (88%)
  matrix products  28.5 us (7%)
  between operations  13.8 us (3%)
  local copies, waits for them, and re-layouts  5.73 us (1%)
    all_gather x1, waiting for transfers between devices, on_device(): up_full = lax.all_gather(w_up, 'rep', axis=0, tiled=True)  84.3 us
    reduce_scatter x1, waiting for transfers between devices, on_device(): lax.psum_scatter(contract_first(cotangent, hidden).astype(jnp.bfloat16),...  76.9 us
    all_gather x1, waiting for transfers between devices, on_device(): lax.all_gather(w_down, 'rep', axis=1, tiled=True)  75 us
    psum x1, waiting for transfers between devices, on_device(): lax.psum(partial_sum, ('fs', 'tp')).astype(jnp.float32).astype(jnp.bfloat16)  63.1 us
    reduce_scatter x1, waiting for transfers between devices, on_device(): lax.psum_scatter(contract_first(hidden_in, slopes).astype(jnp.bfloat16),...  62.8 us
    dot_general x2, matrix products, contract_last(): lax.dot_general(left, right, (((1,), (1,)), ((), ())), preferred_element_...  11.7 us
    dot_general x2, matrix products, contract_first(): lax.dot_general(left, right, (((0,), (0,)), ((), ())), preferred_element_...  10.9 us
  transfers between devices with their start and end apart: 5, of which 5 were waited for; matrix products, arithmetic and copies ran while one was open for 6% of the time, Pallas kernels for 0%

commit v1 on v0

v1 whole, which is shorter than its diff:
```python
import functools

import jax
import jax.numpy as jnp
from jax import lax
from jax.experimental import pallas as pl
from jax.experimental.pallas import tpu as pltpu
from jax.sharding import PartitionSpec as P

BF16 = jnp.bfloat16
F32 = jnp.float32
GATHER_BUDGET = 20 << 20


def contract_last(left, right):
    return lax.dot_general(
        left, right, (((1,), (1,)), ((), ())), preferred_element_type=F32
    )


def contract_first(left, right):
    return lax.dot_general(
        left, right, (((0,), (0,)), ((), ())), preferred_element_type=F32
    )


def swap(value, axis, offset):
    size = lax.axis_size(axis)
    return lax.ppermute(value, axis, [(i, i ^ offset) for i in range(size)])


def gathered_weights(hidden_in, cotangent, w_up, w_down):
    up_full = lax.all_gather(w_up, "rep", axis=0, tiled=True)
    back_grad = contract_last(cotangent, lax.all_gather(w_down, "rep", axis=1, tiled=True))
    preact = jnp.dot(hidden_in, up_full, preferred_element_type=F32)
    active = jnp.maximum(preact, 0.0)
    hidden = (active * active).astype(BF16)
    slopes = (2.0 * active * back_grad).astype(BF16)
    grad_upper = lax.psum_scatter(
        contract_first(hidden_in, slopes).astype(BF16), "rep", scatter_dimension=0, tiled=True
    ).astype(F32)
    lower_rows = lax.psum_scatter(
        contract_first(cotangent, hidden).astype(BF16), "rep", scatter_dimension=0, tiled=True
    ).astype(F32)
    partial_sum = contract_last(slopes, up_full).astype(BF16)
    input_grad = lax.psum(partial_sum, ("fs", "tp"))
    return input_grad, grad_upper, lower_rows.T


def finish(ref, sem):
    pltpu.make_async_copy(ref, ref, sem).wait()


def gather_kernel(mine, theirs, planes, *refs):
    ins = (dict(zip(mine, refs)), dict(zip(theirs, refs[len(mine) :])))
    outs = refs[len(mine) + len(theirs) :][:2]
    sems = refs[-1]
    fs, tp = lax.axis_index("fs"), lax.axis_index("tp")
    part = outs[0].shape[0] // (8 * len(planes))
    for which, name in enumerate(("hidden_in", "cotangent")):
        for core in range(2):
            for k, plane in enumerate(planes):
                for b in range(4):
                    if plane == "own":
                        at = pl.multiple_of(((tp ^ core) * 4 + (fs ^ b)) * part, part)
                        src = ins[0][name].at[pl.ds(at, part), :]
                    elif b < 3:
                        src = ins[core][plane + "oxy"[b]].at[which * part : (which + 1) * part, :]
                    else:
                        src = ins[core][plane + "fg"[which]]
                    to = pl.ds(((core * len(planes) + k) * 4 + b) * part, part)
                    pltpu.make_async_copy(src, outs[which].at[to, :], sems.at[which]).start()
    finish(outs[0], sems.at[0])
    finish(outs[1], sems.at[1])


def gather_rows(mine, theirs, planes):
    tokens, width = mine["hidden_in"].shape
    pieces = [p + k for p in planes if p != "own" for k in "oxyfg"]
    whole = ["hidden_in", "cotangent"]
    any_space = pl.BlockSpec(memory_space=pl.ANY)
    out = pltpu.VMEM((len(planes) * tokens, width), BF16)
    return pl.pallas_call(
        functools.partial(gather_kernel, whole + pieces, pieces, planes),
        out_shape=[out, out],
        in_specs=[any_space] * (2 + 2 * len(pieces)),
        out_specs=[any_space] * 2,
        scratch_shapes=[pltpu.SemaphoreType.DMA((2,))],
        cost_estimate=pl.CostEstimate(flops=4_000_000_000, bytes_accessed=4 * tokens * width * len(planes), transcendentals=0),
        compiler_params=pltpu.CompilerParams(vmem_limit_bytes=1 << 20),
    )(*[mine[k] for k in whole + pieces], *[theirs[k] for k in pieces])


def weights_kernel(w_up, w_down, *refs):
    ups, downs, (up, down, sems) = refs[:3], refs[3:6], refs[6:]
    rep = lax.axis_index("rep")
    shard, cols = w_up.shape[0], up.shape[1]
    for j in range(4):
        at = pl.multiple_of((rep ^ j) * shard, shard)
        mine = pl.multiple_of(rep * cols, cols)
        u = ups[j - 1] if j else w_up.at[:, pl.ds(mine, cols)]
        d = downs[j - 1] if j else w_down.at[pl.ds(mine, cols), :]
        pltpu.make_async_copy(u, up.at[pl.ds(at, shard), :], sems.at[0]).start()
        pltpu.make_async_copy(d, down.at[:, pl.ds(at, shard)], sems.at[1]).start()
    finish(up, sems.at[0])
    finish(down, sems.at[1])


def gather_weights(w_up, w_down, ups, downs):
    (shard, cols), width = ups[0].shape, w_down.shape[1] * 4
    any_space = pl.BlockSpec(memory_space=pl.ANY)
    return pl.pallas_call(
        weights_kernel,
        out_shape=[pltpu.VMEM((width, cols), BF16), pltpu.VMEM((cols, width), BF16)],
        in_specs=[any_space] * 8,
        out_specs=[any_space] * 2,
        scratch_shapes=[pltpu.SemaphoreType.DMA((2,))],
        cost_estimate=pl.CostEstimate(flops=1_000_000_000, bytes_accessed=4 * width * cols, transcendentals=0),
        compiler_params=pltpu.CompilerParams(vmem_limit_bytes=1 << 20),
        name="weights",
    )(w_up, w_down, *ups, *downs)


def gathered_tokens(hidden_in, cotangent, w_up, w_down):
    n_rep, n_fs = lax.axis_size("rep"), lax.axis_size("fs")
    rep, fs, tp = (lax.axis_index(a) for a in ("rep", "fs", "tp"))
    tokens, width = hidden_in.shape
    side = tokens // 2
    part = side // n_fs
    half = width // 2
    shard = w_up.shape[0]
    cols = w_up.shape[1] // n_rep

    def rows_at(value, core, block, count=part):
        return lax.dynamic_slice_in_dim(value, core * side + block * part, count, 0)

    piece = jnp.concatenate([rows_at(hidden_in, tp, fs), rows_at(cotangent, tp, fs)], 0)
    near = swap(piece, "rep", 1)
    far = swap(piece, "rep", 2)
    across = swap(far, "rep", 1)

    ups, downs = [], []
    for j in range(1, n_rep):
        u = lax.dynamic_slice_in_dim(w_up, (rep ^ j) * cols, cols, 1)
        d = lax.dynamic_slice_in_dim(w_down, (rep ^ j) * cols, cols, 0)
        ups.append(swap(u, "rep", j))
        downs.append(swap(d, "rep", j))
    up, down = gather_weights(w_up, w_down, ups, downs)

    mine = dict(hidden_in=hidden_in, cotangent=cotangent)
    theirs = {}
    for plane, own in (("near", near), ("far", far), ("across", across)):
        x = swap(own, "fs", 1)
        y = swap(own, "fs", 2)
        f = swap(x[:part], "fs", 2)
        g = swap(y[part:], "fs", 1)
        for kind, value in zip("oxyfg", (own, x, y, f, g)):
            mine[plane + kind] = value
            theirs[plane + kind] = swap(value, "tp", 1)

    def add(a, b):
        return (a.astype(F32) + b.astype(F32)).astype(BF16)

    def hidden_units(hidden_rows, cot_rows):
        active = jnp.maximum(jnp.dot(hidden_rows, up, preferred_element_type=F32), 0.0)
        back_grad = jnp.dot(cot_rows, down.T, preferred_element_type=F32)
        return (active * active).astype(BF16), (2.0 * active * back_grad).astype(BF16)

    def between_cores(slopes):
        sent = contract_last(slopes[tokens:], up).astype(BF16)
        got = swap(sent, "tp", 1)
        kept = contract_last(slopes[:tokens], up) + got.astype(F32)
        return kept.astype(BF16).reshape(2, n_fs, part, width)

    def over_places(kept):
        left, right = kept[..., :half], kept[..., half:]
        got_left = swap(left[:, 1::2], "fs", 1)
        got_right = swap(right[:, 2:], "fs", 2)
        left, right = add(left[:, ::2], got_left), add(right[:, :2], got_right)
        got_left = swap(left[:, 1], "fs", 2)
        got_right = swap(right[:, 1], "fs", 1)
        return jnp.concatenate([add(left[:, 0], got_left), add(right[:, 0], got_right)], -1)

    h_even, c_even = gather_rows(mine, theirs, ("far", "own"))
    h_odd, c_odd = gather_rows(mine, theirs, ("near", "across"))
    hidden_odd, slopes_odd = hidden_units(h_odd, c_odd)
    kept_odd = between_cores(slopes_odd)
    hidden_even, slopes_even = hidden_units(h_even, c_even)
    kept_even = between_cores(slopes_even)
    odd = over_places(kept_odd)
    even = over_places(kept_even)
    got = swap(odd, "rep", 1)
    own_sum = even[1].astype(F32) + got[0].astype(F32)
    far_sum = add(even[0], got[1])
    final = (own_sum + swap(far_sum, "rep", 2).astype(F32)).astype(BF16)
    blocks = [final] + [swap(final, "fs", b) for b in (1, 2, 3)]
    ours = jnp.zeros((side, width), BF16)
    for b, value in enumerate(blocks):
        ours = lax.dynamic_update_slice_in_dim(ours, value, (fs ^ b) * part, 0)
    others = swap(ours, "tp", 1)
    input_grad = jnp.zeros((tokens, width), BF16)
    input_grad = lax.dynamic_update_slice_in_dim(input_grad, ours, tp * side, 0)
    input_grad = lax.dynamic_update_slice_in_dim(input_grad, others, (1 - tp) * side, 0)

    up_own = (contract_first(h_odd, slopes_odd) + contract_first(h_even, slopes_even)).astype(BF16)
    down_own = (contract_first(hidden_odd, c_odd) + contract_first(hidden_even, c_even)).astype(BF16)
    ups, downs = [], []
    for j in range(n_rep):
        u = lax.dynamic_slice_in_dim(up_own, (rep ^ j) * shard, shard, 0)
        d = lax.dynamic_slice_in_dim(down_own, (rep ^ j) * shard, shard, 1)
        if j:
            u, d = swap(u, "rep", j), swap(d, "rep", j)
        ups.append(u)
        downs.append(d)
    ups, downs, final = lax.optimization_barrier((ups, downs, final))
    up_grad = jnp.zeros((shard, cols * n_rep), F32)
    down_grad = jnp.zeros((cols * n_rep, shard), F32)
    for j in range(n_rep):
        up_grad = lax.dynamic_update_slice_in_dim(up_grad, ups[j].astype(F32), (rep ^ j) * cols, 1)
        down_grad = lax.dynamic_update_slice_in_dim(down_grad, downs[j].astype(F32), (rep ^ j) * cols, 0)
    return input_grad, up_grad, down_grad


def on_device(hidden_in, cotangent, w_up, w_down):
    sizes = tuple(lax.axis_size(a) for a in ("rep", "fs", "tp"))
    gathered = 2 * hidden_in.size * sizes[0] * hidden_in.dtype.itemsize
    fits = sizes == (4, 4, 2) and gathered <= GATHER_BUDGET
    plan = gathered_tokens if fits else gathered_weights
    return plan(hidden_in, cotangent, w_up, w_down)


def solution(mesh):
    return jax.shard_map(
        on_device,
        mesh=mesh,
        in_specs=(P("rep", None), P("rep", None), P("rep", ("fs", "tp")), P(("fs", "tp"), "rep")),
        out_specs=(P("rep", None), P("rep", ("fs", "tp")), P(("fs", "tp"), "rep")),
        check_vma=False,
    )
```

time: 415 us -> 258 us (0.62)
  waiting for transfers between devices: 364 us -> 141 us
  starting transfers between devices: 0.2 us -> 73.6 us
  matrix products: 28.5 us -> 13.4 us
  local copies, waits for them, and re-layouts: 5.73 us -> 19.8 us
  between operations: 13.8 us -> 1.34 us
    all_gather x2 -> x0, waiting for transfers between devices: 159 us -> none  [the longest x1 84.3 us: on_device(): up_full = lax.all_gather(w_up, 'rep', axis=0, tiled=True)]
    ppermute x0 -> x58, waiting for transfers between devices: none -> 141 us  [swap(): return lax.ppermute(value, axis, [(i, i ^ offset) for i in range(size)])]
    reduce_scatter x2 -> x0, waiting for transfers between devices: 140 us -> none  [the longest x1 76.9 us: on_device(): lax.psum_scatter(contract_first(cotangent, hidden).astype(jnp.bfloat16),...]
    ppermute x0 -> x58, starting transfers between devices: none -> 73.6 us  [swap(): return lax.ppermute(value, axis, [(i, i ^ offset) for i in range(size)])]
    psum x1 -> x0, waiting for transfers between devices: 63.1 us -> none  [on_device(): lax.psum(partial_sum, ('fs', 'tp')).astype(jnp.float32).astype(jnp.bfloat16)]
    dot_general x2 -> x4, matrix products: 11.7 us -> 2.96 us  [contract_last(): lax.dot_general(left, right, (((1,), (1,)), ((), ())), preferred_element_...]
    unnamed x4 -> x46, local copies, waits for them, and re-layouts: 5.73 us -> 12.2 us
    dot_general x2 -> x4, matrix products: 10.9 us -> 5.31 us  [contract_first(): lax.dot_general(left, right, (((0,), (0,)), ((), ())), preferred_element_...]
  transfers between devices with their start and end apart: 5 -> 58, of which waited for: 5 -> 24; matrix products, arithmetic and copies ran while one was open for 6% -> 8% of each run, Pallas kernels for 0% -> 2%
where the time goes in v1:
time: 258 us; the launch traced here: 256 us
  waiting for transfers between devices  141 us (55%)
  starting transfers between devices  73.6 us (29%)
  local copies, waits for them, and re-layouts  19.8 us (8%)
  matrix products  13.4 us (5%)
  Pallas kernels  3.87 us (2%)
    ppermute x58, waiting for transfers between devices, swap(): return lax.ppermute(value, axis, [(i, i ^ offset) for i in range(size)])  141 us
    ppermute x58, starting transfers between devices, swap(): return lax.ppermute(value, axis, [(i, i ^ offset) for i in range(size)])  73.6 us
    unnamed x46, local copies, waits for them, and re-layouts  12.2 us
    dot_general x4, matrix products, contract_first(): lax.dot_general(left, right, (((0,), (0,)), ((), ())), preferred_element_...  5.31 us
  transfers between devices with their start and end apart: 58, of which 24 were waited for; matrix products, arithmetic and copies ran while one was open for 8% of the time, Pallas kernels for 2%

profile of v1, /device:TPU:0, one launch (start us, length us, event | category | flops | bytes accessed | tf_op | source)
XLA Modules:
  0.0 255.7 jit_solution(16029273926017620087)
XLA Ops:
  2.7 4.1 %collective-permute-start = (bf16[128,2048]{1,0:T(8,128)(2,1)}, bf16[128,2048]{1,0:T(8,128)(2,1)}, u32[]{:S(2)}, u32[]{:S(2)}) collective-permute-start(bf16[128,2048]{1,0:T(8,128)(2,1)} %pad_maximum_fusion), channel_id=1, source_target_pairs={{0,16},{8,24},{16,0},{24,8},{1,17},{9,25},{17,1},{25,9},{2,18},{10... | collective-permute-start | bytes 1572872 | tf_op jit(solution)/shard_map/ppermute | solution.py:29
  9.0 3.9 %collective-permute-start.12 = (bf16[512,256]{1,0:T(8,128)(2,1)S(1)}, bf16[512,256]{1,0:T(8,128)(2,1)S(1)}, u32[]{:S(2)}, u32[]{:S(2)}) collective-permute-start(bf16[512,256]{1,0:T(8,128)(2,1)S(1)} %get-tuple-element.52), channel_id=1, source_target_pairs={{0,24},{8,16},{16,8},{24,0},{1,25},{9,17},{17,9},{25,1},{2,26},{10... | collective-permute-start | bytes 786440 | tf_op jit(solution)/shard_map/ppermute | solution.py:29
  12.9 18.3 %collective-permute-done.refs_2_ = bf16[128,2048]{1,0:T(8,128)(2,1)} collective-permute-done((bf16[128,2048]{1,0:T(8,128)(2,1)}, bf16[128,2048]{1,0:T(8,128)(2,1)}, u32[]{:S(2)}, u32[]{:S(2)}) %collective-permute-start) | collective-permute-done | bytes 524320 | tf_op jit(solution)/shard_map/ppermute | solution.py:29
  33.1 8.8 %collective-permute-done.10.refs_0_ = bf16[512,256]{1,0:T(8,128)(2,1)S(1)} collective-permute-done((bf16[512,256]{1,0:T(8,128)(2,1)S(1)}, bf16[512,256]{1,0:T(8,128)(2,1)S(1)}, u32[]{:S(2)}, u32[]{:S(2)}) %collective-permute-start.10) | collective-permute-done | bytes 262176 | tf_op jit(solution)/shard_map/ppermute | solution.py:29
  42.6 3.4 %collective-permute-start.14 = (bf16[256,512]{1,0:T(8,128)(2,1)S(1)}, bf16[256,512]{1,0:T(8,128)(2,1)S(1)}, u32[]{:S(2)}, u32[]{:S(2)}) collective-permute-start(bf16[256,512]{1,0:T(8,128)(2,1)S(1)} %get-tuple-element.50), channel_id=1, source_target_pairs={{0,16},{8,24},{16,0},{24,8},{1,17},{9,25},{17,1},{25,9},{2,18},{10... | collective-permute-start | bytes 786440 | tf_op jit(solution)/shard_map/ppermute | solution.py:29
  46.0 3.3 %collective-permute-done.12.refs_2_ = bf16[512,256]{1,0:T(8,128)(2,1)S(1)} collective-permute-done((bf16[512,256]{1,0:T(8,128)(2,1)S(1)}, bf16[512,256]{1,0:T(8,128)(2,1)S(1)}, u32[]{:S(2)}, u32[]{:S(2)}) %collective-permute-start.12) | collective-permute-done | bytes 262176 | tf_op jit(solution)/shard_map/ppermute | solution.py:29
  55.2 4.8 %collective-permute-start.26 = (bf16[128,2048]{1,0:T(8,128)(2,1)}, bf16[128,2048]{1,0:T(8,128)(2,1)S(1)}, u32[]{:S(2)}, u32[]{:S(2)}) collective-permute-start(bf16[128,2048]{1,0:T(8,128)(2,1)} %collective-permute-done.refs_2_), channel_id=1, source_target_pairs={{0,8},{8,0},{16,24},{24,16},{1,9},{9,1},{17,25},{25,17},{2,10},{10... | collective-permute-start | bytes 1572872 | tf_op jit(solution)/shard_map/ppermute | solution.py:29
  60.0 10.4 %collective-permute-done.14.refs_4_ = bf16[256,512]{1,0:T(8,128)(2,1)S(1)} collective-permute-done((bf16[256,512]{1,0:T(8,128)(2,1)S(1)}, bf16[256,512]{1,0:T(8,128)(2,1)S(1)}, u32[]{:S(2)}, u32[]{:S(2)}) %collective-permute-start.14) | collective-permute-done | bytes 262176 | tf_op jit(solution)/shard_map/ppermute | solution.py:29
  76.7 3.8 %collective-permute-done.26.refs_7_ = bf16[128,2048]{1,0:T(8,128)(2,1)S(1)} collective-permute-done((bf16[128,2048]{1,0:T(8,128)(2,1)}, bf16[128,2048]{1,0:T(8,128)(2,1)S(1)}, u32[]{:S(2)}, u32[]{:S(2)}) %collective-permute-start.26) | collective-permute-done | bytes 524320 | tf_op jit(solution)/shard_map/ppermute | solution.py:29
  81.6 4.6 %collective-permute-done.2.refs_4_ = bf16[128,2048]{1,0:T(8,128)(2,1)} collective-permute-done((bf16[128,2048]{1,0:T(8,128)(2,1)}, bf16[128,2048]{1,0:T(8,128)(2,1)}, u32[]{:S(2)}, u32[]{:S(2)}) %collective-permute-start.2) | collective-permute-done | bytes 524320 | tf_op jit(solution)/shard_map/ppermute | solution.py:29
  89.0 8.3 %collective-permute-done.23.refs_4_ = bf16[128,2048]{1,0:T(8,128)(2,1)S(1)} collective-permute-done((bf16[128,2048]{1,0:T(8,128)(2,1)}, bf16[128,2048]{1,0:T(8,128)(2,1)S(1)}, u32[]{:S(2)}, u32[]{:S(2)}) %collective-permute-start.23) | collective-permute-done | bytes 524320 | tf_op jit(solution)/shard_map/ppermute | solution.py:29
  98.7 4.4 %collective-permute-done.3.refs_5_ = bf16[64,2048]{1,0:T(8,128)(2,1)} collective-permute-done((bf16[64,2048]{1,0:T(8,128)(2,1)S(1)}, bf16[64,2048]{1,0:T(8,128)(2,1)}, u32[]{:S(2)}, u32[]{:S(2)}) %collective-permute-start.3) | collective-permute-done | bytes 262176 | tf_op jit(solution)/shard_map/ppermute | solution.py:29
  104.9 4.7 %collective-permute-done.4.refs_6_ = bf16[64,2048]{1,0:T(8,128)(2,1)} collective-permute-done((bf16[64,2048]{1,0:T(8,128)(2,1)S(1)}, bf16[64,2048]{1,0:T(8,128)(2,1)}, u32[]{:S(2)}, u32[]{:S(2)}) %collective-permute-start.4) | collective-permute-done | bytes 262176 | tf_op jit(solution)/shard_map/ppermute | solution.py:29
  127.9 4.0 %collective-permute-done.25.refs_6_ = bf16[64,2048]{1,0:T(8,128)(2,1)S(1)} collective-permute-done((bf16[64,2048]{1,0:T(8,128)(2,1)S(1)}, bf16[64,2048]{1,0:T(8,128)(2,1)S(1)}, u32[]{:S(2)}, u32[]{:S(2)}) %collective-permute-start.25) | collective-permute-done | bytes 262176 | tf_op jit(solution)/shard_map/ppermute | solution.py:29
  135.9 3.7 %collective-permute-done.29.refs_10_ = bf16[64,2048]{1,0:T(8,128)(2,1)S(1)} collective-permute-done((bf16[64,2048]{1,0:T(8,128)(2,1)S(1)}, bf16[64,2048]{1,0:T(8,128)(2,1)S(1)}, u32[]{:S(2)}, u32[]{:S(2)}) %collective-permute-start.29) | collective-permute-done | bytes 262176 | tf_op jit(solution)/shard_map/ppermute | solution.py:29
  157.2 9.3 %collective-permute-done.19 = bf16[2,2,64,1024]{3,2,0,1:T(8,128)(2,1)S(1)} collective-permute-done((bf16[2,2,64,1024]{3,2,0,1:T(8,128)(2,1)S(1)}, bf16[2,2,64,1024]{3,2,0,1:T(8,128)(2,1)S(1)}, u32[]{:S(2)}, u32[]{:S(2)}) %collective-permute-start.19) | collective-permute-done | bytes 524320 | tf_op jit(solution)/shard_map/ppermute | solution.py:29
  168.5 8.7 %collective-permute-done.44 = bf16[2,2,64,1024]{3,2,0,1:T(8,128)(2,1)S(1)} collective-permute-done((bf16[2,2,64,1024]{3,2,0,1:T(8,128)(2,1)S(1)}, bf16[2,2,64,1024]{3,2,0,1:T(8,128)(2,1)S(1)}, u32[]{:S(2)}, u32[]{:S(2)}) %collective-permute-start.44) | collective-permute-done | bytes 524320 | tf_op jit(solution)/shard_map/ppermute | solution.py:29
  181.7 8.0 %collective-permute-done.45 = bf16[2,64,1024]{2,1,0:T(8,128)(2,1)S(1)} collective-permute-done((bf16[2,64,1024]{2,1,0:T(8,128)(2,1)S(1)}, bf16[2,64,1024]{2,1,0:T(8,128)(2,1)S(1)}, u32[]{:S(2)}, u32[]{:S(2)}) %collective-permute-start.45) | collective-permute-done | bytes 262176 | tf_op jit(solution)/shard_map/ppermute | solution.py:29
  192.1 3.1 %collective-permute-start.53 = (bf16[512,256]{1,0:T(8,128)(2,1)S(1)}, bf16[512,256]{1,0:T(8,128)(2,1)S(1)}, u32[]{:S(2)}, u32[]{:S(2)}) collective-permute-start(bf16[512,256]{1,0:T(8,128)(2,1)S(1)} %get-tuple-element.42), channel_id=1, source_target_pairs={{0,16},{8,24},{16,0},{24,8},{1,17},{9,25},{17,1},{25,9},{2,18},{10... | collective-permute-start | bytes 786440 | tf_op jit(solution)/shard_map/ppermute | solution.py:29
  196.8 13.6 %collective-permute-done.46 = bf16[2,64,2048]{2,1,0:T(8,128)(2,1)S(1)} collective-permute-done((bf16[2,64,2048]{2,1,0:T(8,128)(2,1)S(1)}, bf16[2,64,2048]{2,1,0:T(8,128)(2,1)S(1)}, u32[]{:S(2)}, u32[]{:S(2)}) %collective-permute-start.46) | collective-permute-done | bytes 524320 | tf_op jit(solution)/shard_map/ppermute | solution.py:29
  210.4 2.7 %collective-permute-start.47 = (bf16[64,2048]{1,0:T(8,128)(2,1)S(1)}, bf16[64,2048]{1,0:T(8,128)(2,1)S(1)}, u32[]{:S(2)}, u32[]{:S(2)}) collective-permute-start(bf16[64,2048]{1,0:T(8,128)(2,1)S(1)} %fusion.8), channel_id=1, source_target_pairs={{0,16},{8,24},{16,0},{24,8},{1,17},{9,25},{17,1},{25,9},{2,18},{10... | collective-permute-start | bytes 786440 | tf_op jit(solution)/shard_map/ppermute | solution.py:29
  217.5 6.7 %collective-permute-start.56 = (bf16[256,512]{1,0:T(8,128)(2,1)S(1)}, bf16[256,512]{1,0:T(8,128)(2,1)S(1)}, u32[]{:S(2)}, u32[]{:S(2)}) collective-permute-start(bf16[256,512]{1,0:T(8,128)(2,1)S(1)} %get-tuple-element.38), channel_id=1, source_target_pairs={{0,16},{8,24},{16,0},{24,8},{1,17},{9,25},{17,1},{25,9},{2,18},{10... | collective-permute-start | bytes 786440 | tf_op jit(solution)/shard_map/ppermute | solution.py:29
  224.3 11.2 %collective-permute-done.47 = bf16[64,2048]{1,0:T(8,128)(2,1)S(1)} collective-permute-done((bf16[64,2048]{1,0:T(8,128)(2,1)S(1)}, bf16[64,2048]{1,0:T(8,128)(2,1)S(1)}, u32[]{:S(2)}, u32[]{:S(2)}) %collective-permute-start.47) | collective-permute-done | bytes 262176 | tf_op jit(solution)/shard_map/ppermute | solution.py:29
  240.3 10.6 %collective-permute-done.56 = bf16[256,512]{1,0:T(8,128)(2,1)S(1)} collective-permute-done((bf16[256,512]{1,0:T(8,128)(2,1)S(1)}, bf16[256,512]{1,0:T(8,128)(2,1)S(1)}, u32[]{:S(2)}, u32[]{:S(2)}) %collective-permute-start.56) | collective-permute-done | bytes 262176 | tf_op jit(solution)/shard_map/ppermute | solution.py:29
  (203 shorter events, 89.8 us)
Async XLA Ops:
  2.7 28.5 %collective-permute-start = (bf16[128,2048]{1,0:T(8,128)(2,1)}, bf16[128,2048]{1,0:T(8,128)(2,1)}, u32[]{:S(2)}, u32[]{:S(2)}) collective-permute-start(bf16[128,2048]{1,0:T(8,128)(2,1)} %pad_maximum_fusion), channel_id=1, source_target_pairs={{0,16},{8,24},{16,0},{24,8},{1,17},{9,25},{17,1},{25,9},{2,18},{10... | collective-permute-start | bytes 1572872 | tf_op jit(solution)/shard_map/ppermute | solution.py:29
  6.8 45.7 %collective-permute-start.21 = (bf16[128,2048]{1,0:T(8,128)(2,1)}, bf16[128,2048]{1,0:T(8,128)(2,1)}, u32[]{:S(2)}, u32[]{:S(2)}) collective-permute-start(bf16[128,2048]{1,0:T(8,128)(2,1)} %pad_maximum_fusion), channel_id=1, source_target_pairs={{0,8},{8,0},{16,24},{24,16},{1,9},{9,1},{17,25},{25,17},{2,10},{10... | collective-permute-start | bytes 1572872 | tf_op jit(solution)/shard_map/ppermute | solution.py:29
  8.5 33.4 %collective-permute-start.10 = (bf16[512,256]{1,0:T(8,128)(2,1)S(1)}, bf16[512,256]{1,0:T(8,128)(2,1)S(1)}, u32[]{:S(2)}, u32[]{:S(2)}) collective-permute-start(bf16[512,256]{1,0:T(8,128)(2,1)S(1)} %get-tuple-element.54), channel_id=1, source_target_pairs={{0,8},{8,0},{16,24},{24,16},{1,9},{9,1},{17,25},{25,17},{2,10},{10... | collective-permute-start | bytes 786440 | tf_op jit(solution)/shard_map/ppermute | solution.py:29
  9.0 32.9 %collective-permute-start.11 = (bf16[512,256]{1,0:T(8,128)(2,1)S(1)}, bf16[512,256]{1,0:T(8,128)(2,1)S(1)}, u32[]{:S(2)}, u32[]{:S(2)}) collective-permute-start(bf16[512,256]{1,0:T(8,128)(2,1)S(1)} %get-tuple-element.53), channel_id=1, source_target_pairs={{0,16},{8,24},{16,0},{24,8},{1,17},{9,25},{17,1},{25,9},{2,18},{10... | collective-permute-start | bytes 786440 | tf_op jit(solution)/shard_map/ppermute | solution.py:29
  9.0 40.3 %collective-permute-start.12 = (bf16[512,256]{1,0:T(8,128)(2,1)S(1)}, bf16[512,256]{1,0:T(8,128)(2,1)S(1)}, u32[]{:S(2)}, u32[]{:S(2)}) collective-permute-start(bf16[512,256]{1,0:T(8,128)(2,1)S(1)} %get-tuple-element.52), channel_id=1, source_target_pairs={{0,24},{8,16},{16,8},{24,0},{1,25},{9,17},{17,9},{25,1},{2,26},{10... | collective-permute-start | bytes 786440 | tf_op jit(solution)/shard_map/ppermute | solution.py:29
  31.2 42.6 %collective-permute-start.1 = (bf16[128,2048]{1,0:T(8,128)(2,1)}, bf16[128,2048]{1,0:T(8,128)(2,1)}, u32[]{:S(2)}, u32[]{:S(2)}) collective-permute-start(bf16[128,2048]{1,0:T(8,128)(2,1)} %collective-permute-done.refs_2_), channel_id=1, source_target_pairs={{0,2},{2,0},{4,6},{6,4},{1,3},{3,1},{5,7},{7,5},{8,10},{10,8},{12,... | collective-permute-start | bytes 1572872 | tf_op jit(solution)/shard_map/ppermute | solution.py:29
  42.6 27.8 %collective-permute-start.14 = (bf16[256,512]{1,0:T(8,128)(2,1)S(1)}, bf16[256,512]{1,0:T(8,128)(2,1)S(1)}, u32[]{:S(2)}, u32[]{:S(2)}) collective-permute-start(bf16[256,512]{1,0:T(8,128)(2,1)S(1)} %get-tuple-element.50), channel_id=1, source_target_pairs={{0,16},{8,24},{16,0},{24,8},{1,17},{9,25},{17,1},{25,9},{2,18},{10... | collective-permute-start | bytes 786440 | tf_op jit(solution)/shard_map/ppermute | solution.py:29
  50.0 23.0 %collective-permute-start.15 = (bf16[256,512]{1,0:T(8,128)(2,1)S(1)}, bf16[256,512]{1,0:T(8,128)(2,1)S(1)}, u32[]{:S(2)}, u32[]{:S(2)}) collective-permute-start(bf16[256,512]{1,0:T(8,128)(2,1)S(1)} %get-tuple-element.49), channel_id=1, source_target_pairs={{0,24},{8,16},{16,8},{24,0},{1,25},{9,17},{17,9},{25,1},{2,26},{10... | collective-permute-start | bytes 786440 | tf_op jit(solution)/shard_map/ppermute | solution.py:29
  52.5 22.3 %collective-permute-start.22 = (bf16[128,2048]{1,0:T(8,128)(2,1)}, bf16[128,2048]{1,0:T(8,128)(2,1)S(1)}, u32[]{:S(2)}, u32[]{:S(2)}) collective-permute-start(bf16[128,2048]{1,0:T(8,128)(2,1)} %collective-permute-done.21.refs_2_), channel_id=1, source_target_pairs={{0,2},{2,0},{4,6},{6,4},{1,3},{3,1},{5,7},{7,5},{8,10},{10,8},{12,... | collective-permute-start | bytes 1572872 | tf_op jit(solution)/shard_map/ppermute | solution.py:29
  55.2 25.4 %collective-permute-start.26 = (bf16[128,2048]{1,0:T(8,128)(2,1)}, bf16[128,2048]{1,0:T(8,128)(2,1)S(1)}, u32[]{:S(2)}, u32[]{:S(2)}) collective-permute-start(bf16[128,2048]{1,0:T(8,128)(2,1)} %collective-permute-done.refs_2_), channel_id=1, source_target_pairs={{0,8},{8,0},{16,24},{24,16},{1,9},{9,1},{17,25},{25,17},{2,10},{10... | collective-permute-start | bytes 1572872 | tf_op jit(solution)/shard_map/ppermute | solution.py:29
  73.7 23.7 %collective-permute-start.23 = (bf16[128,2048]{1,0:T(8,128)(2,1)}, bf16[128,2048]{1,0:T(8,128)(2,1)S(1)}, u32[]{:S(2)}, u32[]{:S(2)}) collective-permute-start(bf16[128,2048]{1,0:T(8,128)(2,1)} %collective-permute-done.21.refs_2_), channel_id=1, source_target_pairs={{0,4},{2,6},{4,0},{6,2},{1,5},{3,7},{5,1},{7,3},{8,12},{10,14},{12... | collective-permute-start | bytes 1572872 | tf_op jit(solution)/shard_map/ppermute | solution.py:29
  73.9 23.5 %collective-permute-start.5 = (bf16[128,2048]{1,0:T(8,128)(2,1)}, bf16[128,2048]{1,0:T(8,128)(2,1)S(1)}, u32[]{:S(2)}, u32[]{:S(2)}) collective-permute-start(bf16[128,2048]{1,0:T(8,128)(2,1)} %collective-permute-done.refs_2_), channel_id=1, source_target_pairs={{0,1},{1,0},{2,3},{3,2},{4,5},{5,4},{6,7},{7,6},{8,9},{9,8},{10,11... | collective-permute-start | bytes 1572872 | tf_op jit(solution)/shard_map/ppermute | solution.py:29
  74.8 28.3 %collective-permute-start.3 = (bf16[64,2048]{1,0:T(8,128)(2,1)S(1)}, bf16[64,2048]{1,0:T(8,128)(2,1)}, u32[]{:S(2)}, u32[]{:S(2)}) collective-permute-start(bf16[64,2048]{1,0:T(8,128)(2,1)S(1)} %slice.134), channel_id=1, source_target_pairs={{0,4},{2,6},{4,0},{6,2},{1,5},{3,7},{5,1},{7,3},{8,12},{10,14},{12... | collective-permute-start | bytes 786440 | tf_op jit(solution)/shard_map/ppermute | solution.py:29
  80.6 29.0 %collective-permute-start.27 = (bf16[128,2048]{1,0:T(8,128)(2,1)S(1)}, bf16[128,2048]{1,0:T(8,128)(2,1)}, u32[]{:S(2)}, u32[]{:S(2)}) collective-permute-start(bf16[128,2048]{1,0:T(8,128)(2,1)S(1)} %collective-permute-done.26.refs_7_), channel_id=1, source_target_pairs={{0,2},{2,0},{4,6},{6,4},{1,3},{3,1},{5,7},{7,5},{8,10},{10,8},{12,... | collective-permute-start | bytes 1572872 | tf_op jit(solution)/shard_map/ppermute | solution.py:29
  86.2 25.5 %collective-permute-start.28 = (bf16[128,2048]{1,0:T(8,128)(2,1)S(1)}, bf16[128,2048]{1,0:T(8,128)(2,1)}, u32[]{:S(2)}, u32[]{:S(2)}) collective-permute-start(bf16[128,2048]{1,0:T(8,128)(2,1)S(1)} %collective-permute-done.26.refs_7_), channel_id=1, source_target_pairs={{0,4},{2,6},{4,0},{6,2},{1,5},{3,7},{5,1},{7,3},{8,12},{10,14},{12... | collective-permute-start | bytes 1572872 | tf_op jit(solution)/shard_map/ppermute | solution.py:29
  98.2 22.4 %collective-permute-start.7 = (bf16[128,2048]{1,0:T(8,128)(2,1)}, bf16[128,2048]{1,0:T(8,128)(2,1)}, u32[]{:S(2)}, u32[]{:S(2)}) collective-permute-start(bf16[128,2048]{1,0:T(8,128)(2,1)} %collective-permute-done.2.refs_4_), channel_id=1, source_target_pairs={{0,1},{1,0},{2,3},{3,2},{4,5},{5,4},{6,7},{7,6},{8,9},{9,8},{10,11... | collective-permute-start | bytes 1572872 | tf_op jit(solution)/shard_map/ppermute | solution.py:29
  156.6 22.7 %collective-permute-start.42 = (bf16[2,2,64,1024]{3,2,0,1:T(8,128)(2,1)S(1)}, bf16[2,2,64,1024]{3,2,0,1:T(8,128)(2,1)S(1)}, u32[]{:S(2)}, u32[]{:S(2)}) collective-permute-start(bf16[2,2,64,1024]{3,2,0,1:T(8,128)(2,1)S(1)} %copy.20), channel_id=1, source_target_pairs={{0,2},{2,0},{4,6},{6,4},{1,3},{3,1},{5,7},{7,5},{8,10},{10,8},{12,... | collective-permute-start | bytes 1572872 | tf_op jit(solution)/shard_map/ppermute | solution.py:29
  166.8 28.4 %collective-permute-start.20 = (bf16[2,64,1024]{2,1,0:T(8,128)(2,1)S(1)}, bf16[2,64,1024]{2,1,0:T(8,128)(2,1)S(1)}, u32[]{:S(2)}, u32[]{:S(2)}) collective-permute-start(bf16[2,64,1024]{2,1,0:T(8,128)(2,1)S(1)} %slice_bitcast_fusion.4), channel_id=1, source_target_pairs={{0,2},{2,0},{4,6},{6,4},{1,3},{3,1},{5,7},{7,5},{8,10},{10,8},{12,... | collective-permute-start | bytes 786440 | tf_op jit(solution)/shard_map/ppermute | solution.py:29
  191.7 25.8 %collective-permute-start.52 = (bf16[512,256]{1,0:T(8,128)(2,1)S(1)}, bf16[512,256]{1,0:T(8,128)(2,1)S(1)}, u32[]{:S(2)}, u32[]{:S(2)}) collective-permute-start(bf16[512,256]{1,0:T(8,128)(2,1)S(1)} %get-tuple-element.43), channel_id=1, source_target_pairs={{0,8},{8,0},{16,24},{24,16},{1,9},{9,1},{17,25},{25,17},{2,10},{10... | collective-permute-start | bytes 786440 | tf_op jit(solution)/shard_map/ppermute | solution.py:29
  192.1 44.6 %collective-permute-start.53 = (bf16[512,256]{1,0:T(8,128)(2,1)S(1)}, bf16[512,256]{1,0:T(8,128)(2,1)S(1)}, u32[]{:S(2)}, u32[]{:S(2)}) collective-permute-start(bf16[512,256]{1,0:T(8,128)(2,1)S(1)} %get-tuple-element.42), channel_id=1, source_target_pairs={{0,16},{8,24},{16,0},{24,8},{1,17},{9,25},{17,1},{25,9},{2,18},{10... | collective-permute-start | bytes 786440 | tf_op jit(solution)/shard_map/ppermute | solution.py:29
  195.2 43.1 %collective-permute-start.54 = (bf16[512,256]{1,0:T(8,128)(2,1)S(1)}, bf16[512,256]{1,0:T(8,128)(2,1)S(1)}, u32[]{:S(2)}, u32[]{:S(2)}) collective-permute-start(bf16[512,256]{1,0:T(8,128)(2,1)S(1)} %get-tuple-element.41), channel_id=1, source_target_pairs={{0,24},{8,16},{16,8},{24,0},{1,25},{9,17},{17,9},{25,1},{2,26},{10... | collective-permute-start | bytes 786440 | tf_op jit(solution)/shard_map/ppermute | solution.py:29
  210.4 25.0 %collective-permute-start.47 = (bf16[64,2048]{1,0:T(8,128)(2,1)S(1)}, bf16[64,2048]{1,0:T(8,128)(2,1)S(1)}, u32[]{:S(2)}, u32[]{:S(2)}) collective-permute-start(bf16[64,2048]{1,0:T(8,128)(2,1)S(1)} %fusion.8), channel_id=1, source_target_pairs={{0,16},{8,24},{16,0},{24,8},{1,17},{9,25},{17,1},{25,9},{2,18},{10... | collective-permute-start | bytes 786440 | tf_op jit(solution)/shard_map/ppermute | solution.py:29
  214.5 24.5 %collective-permute-start.55 = (bf16[256,512]{1,0:T(8,128)(2,1)S(1)}, bf16[256,512]{1,0:T(8,128)(2,1)S(1)}, u32[]{:S(2)}, u32[]{:S(2)}) collective-permute-start(bf16[256,512]{1,0:T(8,128)(2,1)S(1)} %get-tuple-element.39), channel_id=1, source_target_pairs={{0,8},{8,0},{16,24},{24,16},{1,9},{9,1},{17,25},{25,17},{2,10},{10... | collective-permute-start | bytes 786440 | tf_op jit(solution)/shard_map/ppermute | solution.py:29
  217.5 33.3 %collective-permute-start.56 = (bf16[256,512]{1,0:T(8,128)(2,1)S(1)}, bf16[256,512]{1,0:T(8,128)(2,1)S(1)}, u32[]{:S(2)}, u32[]{:S(2)}) collective-permute-start(bf16[256,512]{1,0:T(8,128)(2,1)S(1)} %get-tuple-element.38), channel_id=1, source_target_pairs={{0,16},{8,24},{16,0},{24,8},{1,17},{9,25},{17,1},{25,9},{2,18},{10... | collective-permute-start | bytes 786440 | tf_op jit(solution)/shard_map/ppermute | solution.py:29
  (55 other events, 468.0 us)

commit v2 on v1

--- a/solution.py
+++ b/solution.py
@@ -64,6 +64,8 @@
                     if plane == "own":
                         at = pl.multiple_of(((tp ^ core) * 4 + (fs ^ b)) * part, part)
                         src = ins[0][name].at[pl.ds(at, part), :]
+                    elif b < 3 and plane == "near":
+                        src = ins[core][plane + "oxy"[b] + "hc"[which]]
                     elif b < 3:
                         src = ins[core][plane + "oxy"[b]].at[which * part : (which + 1) * part, :]
                     else:
@@ -74,16 +76,31 @@
     finish(outs[1], sems.at[1])
 
 
+def cut(value, at, count, dim):
+    starts = [at if d == dim else 0 for d in range(2)]
+    sizes = [count if d == dim else n for d, n in enumerate(value.shape)]
+    return lax.dynamic_slice(value, starts, sizes, allow_negative_indices=False)
+
+
+def put(into, value, at, dim):
+    starts = [at if d == dim else 0 for d in range(2)]
+    return lax.dynamic_update_slice(into, value, starts, allow_negative_indices=False)
+
+
+def theirs_of(pieces, planes):
+    return [name for name in pieces if name.startswith(planes)]
+
+
 def gather_rows(mine, theirs, planes):
     tokens, width = mine["hidden_in"].shape
-    pieces = [p + k for p in planes if p != "own" for k in "oxyfg"]
+    pieces = list(theirs_of(theirs, planes))
     whole = ["hidden_in", "cotangent"]
     any_space = pl.BlockSpec(memory_space=pl.ANY)
     out = pltpu.VMEM((len(planes) * tokens, width), BF16)
     return pl.pallas_call(
         functools.partial(gather_kernel, whole + pieces, pieces, planes),
         out_shape=[out, out],
-        in_specs=[any_space] * (2 + 2 * len(pieces)),
+        in_specs=[pl.BlockSpec(memory_space=pltpu.HBM)] * 2 + [any_space] * (2 * len(pieces)),
         out_specs=[any_space] * 2,
         scratch_shapes=[pltpu.SemaphoreType.DMA((2,))],
         cost_estimate=pl.CostEstimate(flops=4_000_000_000, bytes_accessed=4 * tokens * width * len(planes), transcendentals=0),
@@ -112,7 +129,7 @@
     return pl.pallas_call(
         weights_kernel,
         out_shape=[pltpu.VMEM((width, cols), BF16), pltpu.VMEM((cols, width), BF16)],
-        in_specs=[any_space] * 8,
+        in_specs=[pl.BlockSpec(memory_space=pltpu.HBM)] * 2 + [any_space] * 6,
         out_specs=[any_space] * 2,
         scratch_shapes=[pltpu.SemaphoreType.DMA((2,))],
         cost_estimate=pl.CostEstimate(flops=1_000_000_000, bytes_accessed=4 * width * cols, transcendentals=0),
@@ -131,32 +148,48 @@
     shard = w_up.shape[0]
     cols = w_up.shape[1] // n_rep
 
-    def rows_at(value, core, block, count=part):
-        return lax.dynamic_slice_in_dim(value, core * side + block * part, count, 0)
-
-    piece = jnp.concatenate([rows_at(hidden_in, tp, fs), rows_at(cotangent, tp, fs)], 0)
-    near = swap(piece, "rep", 1)
-    far = swap(piece, "rep", 2)
+    at_shard = [(rep ^ j) * shard for j in range(n_rep)]
+    at_cols = [(rep ^ j) * cols for j in range(n_rep)]
+    at_block = [(fs ^ b) * part for b in range(n_fs)]
+    at_side = [tp * side, (1 - tp) * side]
+
+    at_own = at_side[0] + at_block[0]
+    own_h, own_c = cut(hidden_in, at_own, part, 0), cut(cotangent, at_own, part, 0)
+    near_h = swap(own_h, "rep", 1)
+    near_c = swap(own_c, "rep", 1)
+    far = swap(jnp.concatenate([own_h, own_c], 0), "rep", 2)
     across = swap(far, "rep", 1)
 
     ups, downs = [], []
     for j in range(1, n_rep):
-        u = lax.dynamic_slice_in_dim(w_up, (rep ^ j) * cols, cols, 1)
-        d = lax.dynamic_slice_in_dim(w_down, (rep ^ j) * cols, cols, 0)
+        u = cut(w_up, at_cols[j], cols, 1)
+        d = cut(w_down, at_cols[j], cols, 0)
         ups.append(swap(u, "rep", j))
         downs.append(swap(d, "rep", j))
+    near_h, at_shard = lax.optimization_barrier((near_h, at_shard))
     up, down = gather_weights(w_up, w_down, ups, downs)
 
     mine = dict(hidden_in=hidden_in, cotangent=cotangent)
     theirs = {}
-    for plane, own in (("near", near), ("far", far), ("across", across)):
+
+    def keep(name, value):
+        mine[name] = value
+        theirs[name] = swap(value, "tp", 1)
+
+    for own, kind in ((near_h, "h"), (near_c, "c")):
+        x = swap(own, "fs", 1)
+        y = swap(own, "fs", 2)
+        f = swap(x if kind == "h" else y, "fs", 2 if kind == "h" else 1)
+        for name, value in (("o", own), ("x", x), ("y", y)):
+            keep("near" + name + kind, value)
+        keep("near" + ("f" if kind == "h" else "g"), f)
+    for plane, own in (("far", far), ("across", across)):
         x = swap(own, "fs", 1)
         y = swap(own, "fs", 2)
         f = swap(x[:part], "fs", 2)
         g = swap(y[part:], "fs", 1)
         for kind, value in zip("oxyfg", (own, x, y, f, g)):
-            mine[plane + kind] = value
-            theirs[plane + kind] = swap(value, "tp", 1)
+            keep(plane + kind, value)
 
     def add(a, b):
         return (a.astype(F32) + b.astype(F32)).astype(BF16)
@@ -181,33 +214,32 @@
         got_right = swap(right[:, 1], "fs", 1)
         return jnp.concatenate([add(left[:, 0], got_left), add(right[:, 0], got_right)], -1)
 
-    h_even, c_even = gather_rows(mine, theirs, ("far", "own"))
-    h_odd, c_odd = gather_rows(mine, theirs, ("near", "across"))
-    hidden_odd, slopes_odd = hidden_units(h_odd, c_odd)
-    kept_odd = between_cores(slopes_odd)
-    hidden_even, slopes_even = hidden_units(h_even, c_even)
-    kept_even = between_cores(slopes_even)
-    odd = over_places(kept_odd)
-    even = over_places(kept_even)
-    got = swap(odd, "rep", 1)
-    own_sum = even[1].astype(F32) + got[0].astype(F32)
-    far_sum = add(even[0], got[1])
-    final = (own_sum + swap(far_sum, "rep", 2).astype(F32)).astype(BF16)
+    h_first, c_first = gather_rows(mine, theirs, ("near", "far"))
+    h_last, c_last = gather_rows(mine, theirs, ("across", "own"))
+    hidden_first, slopes_first = hidden_units(h_first, c_first)
+    kept_first = between_cores(slopes_first)
+    hidden_last, slopes_last = hidden_units(h_last, c_last)
+    kept_last = between_cores(slopes_last)
+    first = over_places(kept_first)
+    last = over_places(kept_last)
+    got = swap(first, "rep", 1)
+    own_sum = last[1].astype(F32) + got[0].astype(F32)
+    across_sum = add(last[0], got[1])
+    final = (own_sum + swap(across_sum, "rep", 3).astype(F32)).astype(BF16)
     blocks = [final] + [swap(final, "fs", b) for b in (1, 2, 3)]
     ours = jnp.zeros((side, width), BF16)
     for b, value in enumerate(blocks):
-        ours = lax.dynamic_update_slice_in_dim(ours, value, (fs ^ b) * part, 0)
+        ours = put(ours, value, at_block[b], 0)
     others = swap(ours, "tp", 1)
     input_grad = jnp.zeros((tokens, width), BF16)
-    input_grad = lax.dynamic_update_slice_in_dim(input_grad, ours, tp * side, 0)
-    input_grad = lax.dynamic_update_slice_in_dim(input_grad, others, (1 - tp) * side, 0)
-
-    up_own = (contract_first(h_odd, slopes_odd) + contract_first(h_even, slopes_even)).astype(BF16)
-    down_own = (contract_first(hidden_odd, c_odd) + contract_first(hidden_even, c_even)).astype(BF16)
+    input_grad = put(put(input_grad, ours, at_side[0], 0), others, at_side[1], 0)
+
+    up_own = (contract_first(h_first, slopes_first) + contract_first(h_last, slopes_last)).astype(BF16)
+    down_own = (contract_first(hidden_first, c_first) + contract_first(hidden_last, c_last)).astype(BF16)
     ups, downs = [], []
     for j in range(n_rep):
-        u = lax.dynamic_slice_in_dim(up_own, (rep ^ j) * shard, shard, 0)
-        d = lax.dynamic_slice_in_dim(down_own, (rep ^ j) * shard, shard, 1)
+        u = cut(up_own, at_shard[j], shard, 0)
+        d = cut(down_own, at_shard[j], shard, 1)
         if j:
             u, d = swap(u, "rep", j), swap(d, "rep", j)
         ups.append(u)
@@ -216,8 +248,8 @@
     up_grad = jnp.zeros((shard, cols * n_rep), F32)
     down_grad = jnp.zeros((cols * n_rep, shard), F32)
     for j in range(n_rep):
-        up_grad = lax.dynamic_update_slice_in_dim(up_grad, ups[j].astype(F32), (rep ^ j) * cols, 1)
-        down_grad = lax.dynamic_update_slice_in_dim(down_grad, downs[j].astype(F32), (rep ^ j) * cols, 0)
+        up_grad = put(up_grad, ups[j].astype(F32), at_cols[j], 1)
+        down_grad = put(down_grad, downs[j].astype(F32), at_cols[j], 0)
     return input_grad, up_grad, down_grad
 
 

time: 258 us -> 270 us (1.047)
  local copies, waits for them, and re-layouts: 19.8 us -> 46.9 us
  waiting for transfers between devices: 141 us -> 115 us
  starting transfers between devices: 73.6 us -> 81.9 us
    ppermute x58 -> x64, waiting for transfers between devices: 141 us -> 115 us  [swap(): return lax.ppermute(value, axis, [(i, i ^ offset) for i in range(size)])]
    unnamed x46 -> x102, local copies, waits for them, and re-layouts: 12.2 us -> 36.4 us
    ppermute x58 -> x64, starting transfers between devices: 73.6 us -> 81.9 us  [swap(): return lax.ppermute(value, axis, [(i, i ^ offset) for i in range(size)])]
    dynamic_slice x5 -> x6, local copies, waits for them, and re-layouts: 1.56 us -> 6.51 us  [cut(): return lax.dynamic_slice(value, starts, sizes, allow_negative_indices=False)]
  transfers between devices with their start and end apart: 58 -> 64, of which waited for: 24 -> 20; matrix products, arithmetic and copies ran while one was open for 8% -> 10% of each run, Pallas kernels for 2% -> 1%
where the time goes in v2:
time: 270 us; the launch traced here: 265 us
  waiting for transfers between devices  115 us (43%)
  starting transfers between devices  81.9 us (30%)
  local copies, waits for them, and re-layouts  46.9 us (17%)
  matrix products  13.6 us (5%)
  Pallas kernels  3.62 us (1%)
  other arithmetic  3.48 us (1%)
    ppermute x64, waiting for transfers between devices, swap(): return lax.ppermute(value, axis, [(i, i ^ offset) for i in range(size)])  115 us
    ppermute x64, starting transfers between devices, swap(): return lax.ppermute(value, axis, [(i, i ^ offset) for i in range(size)])  81.9 us
    unnamed x102, local copies, waits for them, and re-layouts  36.4 us
    dynamic_slice x6, local copies, waits for them, and re-layouts, cut(): return lax.dynamic_slice(value, starts, sizes, allow_negative_indices=False)  6.51 us
    dot_general x4, matrix products, contract_first(): lax.dot_general(left, right, (((0,), (0,)), ((), ())), preferred_element_...  5.57 us
  transfers between devices with their start and end apart: 64, of which 20 were waited for; matrix products, arithmetic and copies ran while one was open for 10% of the time, Pallas kernels for 1%

profile of v2, /device:TPU:0, one launch (start us, length us, event | category | flops | bytes accessed | tf_op | source)
XLA Modules:
  0.0 265.4 jit_solution(7957560195864884142)
XLA Ops:
  2.8 3.1 %collective-permute-start.11 = (bf16[512,256]{1,0:T(8,128)(2,1)}, bf16[512,256]{1,0:T(8,128)(2,1)S(1)}, u32[]{:S(2)}, u32[]{:S(2)}) collective-permute-start(bf16[512,256]{1,0:T(8,128)(2,1)} %get-tuple-element.64), channel_id=1, source_target_pairs={{0,8},{8,0},{16,24},{24,16},{1,9},{9,1},{17,25},{25,17},{2,10},{10... | collective-permute-start | bytes 786440 | tf_op jit(solution)/shard_map/ppermute | solution.py:29
  5.8 2.6 collective-permute-start.12
  15.9 2.2 collective-permute-done.11.refs_0_
  18.8 2.2 collective-permute-start.15
  21.0 6.4 %collective-permute-done.12.refs_1_ = bf16[512,256]{1,0:T(8,128)(2,1)S(1)} collective-permute-done((bf16[512,256]{1,0:T(8,128)(2,1)}, bf16[512,256]{1,0:T(8,128)(2,1)S(1)}, u32[]{:S(2)}, u32[]{:S(2)}) %collective-permute-start.12) | collective-permute-done | bytes 262176 | tf_op jit(solution)/shard_map/ppermute | solution.py:29
  28.8 6.5 %collective-permute-start = (bf16[128,2048]{1,0:T(8,128)(2,1)}, bf16[128,2048]{1,0:T(8,128)(2,1)}, u32[]{:S(2)}, u32[]{:S(2)}) collective-permute-start(bf16[128,2048]{1,0:T(8,128)(2,1)} %pad_maximum_fusion), channel_id=1, source_target_pairs={{0,16},{8,24},{16,0},{24,8},{1,17},{9,25},{17,1},{25,9},{2,18},{10... | collective-permute-start | bytes 1572872 | tf_op jit(solution)/shard_map/ppermute | solution.py:29
  35.3 5.9 %collective-permute-done.22.refs_2_ = bf16[64,2048]{1,0:T(8,128)(2,1)S(1)} collective-permute-done((bf16[64,2048]{1,0:T(8,128)(2,1)S(1)}, bf16[64,2048]{1,0:T(8,128)(2,1)S(1)}, u32[]{:S(2)}, u32[]{:S(2)}) %collective-permute-start.22) | collective-permute-done | bytes 262176 | tf_op jit(solution)/shard_map/ppermute | solution.py:29
  41.2 3.9 %collective-permute-start.16 = (bf16[256,512]{1,0:T(8,128)(2,1)}, bf16[256,512]{1,0:T(8,128)(2,1)S(1)}, u32[]{:S(2)}, u32[]{:S(2)}) collective-permute-start(bf16[256,512]{1,0:T(8,128)(2,1)} %get-tuple-element.59), channel_id=1, source_target_pairs={{0,24},{8,16},{16,8},{24,0},{1,25},{9,17},{17,9},{25,1},{2,26},{10... | collective-permute-start | bytes 786440 | tf_op jit(solution)/shard_map/ppermute | solution.py:29
  49.5 2.1 collective-permute-done.26.refs_6_
  53.3 12.0 %collective-permute-done.16.refs_5_ = bf16[256,512]{1,0:T(8,128)(2,1)S(1)} collective-permute-done((bf16[256,512]{1,0:T(8,128)(2,1)}, bf16[256,512]{1,0:T(8,128)(2,1)S(1)}, u32[]{:S(2)}, u32[]{:S(2)}) %collective-permute-start.16) | collective-permute-done | bytes 262176 | tf_op jit(solution)/shard_map/ppermute | solution.py:29
  68.1 4.4 %collective-permute-done.refs_10_ = bf16[128,2048]{1,0:T(8,128)(2,1)} collective-permute-done((bf16[128,2048]{1,0:T(8,128)(2,1)}, bf16[128,2048]{1,0:T(8,128)(2,1)}, u32[]{:S(2)}, u32[]{:S(2)}) %collective-permute-start) | collective-permute-done | bytes 524320 | tf_op jit(solution)/shard_map/ppermute | solution.py:29
  79.1 4.1 %collective-permute-done.25.refs_5_ = bf16[64,2048]{1,0:T(8,128)(2,1)S(1)} collective-permute-done((bf16[64,2048]{1,0:T(8,128)(2,1)S(1)}, bf16[64,2048]{1,0:T(8,128)(2,1)S(1)}, u32[]{:S(2)}, u32[]{:S(2)}) %collective-permute-start.25) | collective-permute-done | bytes 262176 | tf_op jit(solution)/shard_map/ppermute | solution.py:29
  83.2 9.3 %collective-permute-start.1 = (bf16[128,2048]{1,0:T(8,128)(2,1)}, bf16[128,2048]{1,0:T(8,128)(2,1)S(1)}, u32[]{:S(2)}, u32[]{:S(2)}) collective-permute-start(bf16[128,2048]{1,0:T(8,128)(2,1)} %collective-permute-done.refs_10_), channel_id=1, source_target_pairs={{0,8},{8,0},{16,24},{24,16},{1,9},{9,1},{17,25},{25,17},{2,10},{10... | collective-permute-start | bytes 1572872 | tf_op jit(solution)/shard_map/ppermute | solution.py:29
  108.4 2.9 %collective-permute-done.33.refs_14_ = bf16[64,2048]{1,0:T(8,128)(2,1)} collective-permute-done((bf16[64,2048]{1,0:T(8,128)(2,1)S(1)}, bf16[64,2048]{1,0:T(8,128)(2,1)}, u32[]{:S(2)}, u32[]{:S(2)}) %collective-permute-start.33) | collective-permute-done | bytes 262176 | tf_op jit(solution)/shard_map/ppermute | solution.py:29
  111.3 10.5 %collective-permute-done.2.refs_3_ = bf16[128,2048]{1,0:T(8,128)(2,1)} collective-permute-done((bf16[128,2048]{1,0:T(8,128)(2,1)S(1)}, bf16[128,2048]{1,0:T(8,128)(2,1)}, u32[]{:S(2)}, u32[]{:S(2)}) %collective-permute-start.2) | collective-permute-done | bytes 524320 | tf_op jit(solution)/shard_map/ppermute | solution.py:29
  165.4 10.6 %collective-permute-done.50 = bf16[2,2,64,1024]{3,2,0,1:T(8,128)(2,1)S(1)} collective-permute-done((bf16[2,2,64,1024]{3,2,0,1:T(8,128)(2,1)S(1)}, bf16[2,2,64,1024]{3,2,0,1:T(8,128)(2,1)S(1)}, u32[]{:S(2)}, u32[]{:S(2)}) %collective-permute-start.50) | collective-permute-done | bytes 524320 | tf_op jit(solution)/shard_map/ppermute | solution.py:29
  182.5 2.9 %collective-permute-done.51 = bf16[2,64,1024]{2,1,0:T(8,128)(2,1)S(1)} collective-permute-done((bf16[2,64,1024]{2,1,0:T(8,128)(2,1)S(1)}, bf16[2,64,1024]{2,1,0:T(8,128)(2,1)S(1)}, u32[]{:S(2)}, u32[]{:S(2)}) %collective-permute-start.51) | collective-permute-done | bytes 262176 | tf_op jit(solution)/shard_map/ppermute | solution.py:29
  185.5 3.2 %collective-permute-done.49 = bf16[2,64,1024]{2,1,0:T(8,128)(2,1)S(1)} collective-permute-done((bf16[2,64,1024]{2,1,0:T(8,128)(2,1)S(1)}, bf16[2,64,1024]{2,1,0:T(8,128)(2,1)S(1)}, u32[]{:S(2)}, u32[]{:S(2)}) %collective-permute-start.49) | collective-permute-done | bytes 262176 | tf_op jit(solution)/shard_map/ppermute | solution.py:29
  188.8 5.4 %collective-permute-start.52 = (bf16[2,64,2048]{2,1,0:T(8,128)(2,1)S(1)}, bf16[2,64,2048]{2,1,0:T(8,128)(2,1)S(1)}, u32[]{:S(2)}, u32[]{:S(2)}) collective-permute-start(bf16[2,64,2048]{2,1,0:T(8,128)(2,1)S(1)} %pad_maximum_fusion.1), channel_id=1, source_target_pairs={{0,8},{8,0},{16,24},{24,16},{1,9},{9,1},{17,25},{25,17},{2,10},{10... | collective-permute-start | bytes 1572872 | tf_op jit(solution)/shard_map/ppermute | solution.py:29
  194.2 3.6 %collective-permute-done.20 = bf16[2,2,64,1024]{3,2,0,1:T(8,128)(2,1)S(1)} collective-permute-done((bf16[2,2,64,1024]{3,2,0,1:T(8,128)(2,1)S(1)}, bf16[2,2,64,1024]{3,2,0,1:T(8,128)(2,1)S(1)}, u32[]{:S(2)}, u32[]{:S(2)}) %collective-permute-start.20) | collective-permute-done | bytes 524320 | tf_op jit(solution)/shard_map/ppermute | solution.py:29
  200.6 5.9 %collective-permute-start.58 = (bf16[512,256]{1,0:T(8,128)(2,1)S(1)}, bf16[512,256]{1,0:T(8,128)(2,1)S(1)}, u32[]{:S(2)}, u32[]{:S(2)}) collective-permute-start(bf16[512,256]{1,0:T(8,128)(2,1)S(1)} %get-tuple-element.53), channel_id=1, source_target_pairs={{0,8},{8,0},{16,24},{24,16},{1,9},{9,1},{17,25},{25,17},{2,10},{10... | collective-permute-start | bytes 786440 | tf_op jit(solution)/shard_map/ppermute | solution.py:29
  209.2 2.5 collective-permute-start.53
  216.8 16.2 %collective-permute-done.53 = bf16[64,2048]{1,0:T(8,128)(2,1)S(1)} collective-permute-done((bf16[64,2048]{1,0:T(8,128)(2,1)S(1)}, bf16[64,2048]{1,0:T(8,128)(2,1)S(1)}, u32[]{:S(2)}, u32[]{:S(2)}) %collective-permute-start.53) | collective-permute-done | bytes 262176 | tf_op jit(solution)/shard_map/ppermute | solution.py:29
  238.1 22.5 %collective-permute-done.62 = bf16[256,512]{1,0:T(8,128)(2,1)S(1)} collective-permute-done((bf16[256,512]{1,0:T(8,128)(2,1)S(1)}, bf16[256,512]{1,0:T(8,128)(2,1)S(1)}, u32[]{:S(2)}, u32[]{:S(2)}) %collective-permute-start.62) | collective-permute-done | bytes 262176 | tf_op jit(solution)/shard_map/ppermute | solution.py:29
  (270 shorter events, 113.4 us)
Async XLA Ops:
  5.8 21.6 %collective-permute-start.12 = (bf16[512,256]{1,0:T(8,128)(2,1)}, bf16[512,256]{1,0:T(8,128)(2,1)S(1)}, u32[]{:S(2)}, u32[]{:S(2)}) collective-permute-start(bf16[512,256]{1,0:T(8,128)(2,1)} %get-tuple-element.63), channel_id=1, source_target_pairs={{0,16},{8,24},{16,0},{24,8},{1,17},{9,25},{17,1},{25,9},{2,18},{10... | collective-permute-start | bytes 786440 | tf_op jit(solution)/shard_map/ppermute | solution.py:29
  9.4 35.7 %collective-permute-start.14 = (bf16[256,512]{1,0:T(8,128)(2,1)}, bf16[256,512]{1,0:T(8,128)(2,1)S(1)}, u32[]{:S(2)}, u32[]{:S(2)}) collective-permute-start(bf16[256,512]{1,0:T(8,128)(2,1)} %get-tuple-element.61), channel_id=1, source_target_pairs={{0,8},{8,0},{16,24},{24,16},{1,9},{9,1},{17,25},{25,17},{2,10},{10... | collective-permute-start | bytes 786440 | tf_op jit(solution)/shard_map/ppermute | solution.py:29
  11.2 29.9 %collective-permute-start.22 = (bf16[64,2048]{1,0:T(8,128)(2,1)S(1)}, bf16[64,2048]{1,0:T(8,128)(2,1)S(1)}, u32[]{:S(2)}, u32[]{:S(2)}) collective-permute-start(bf16[64,2048]{1,0:T(8,128)(2,1)S(1)} %constant_dynamic-slice_fusion.15), channel_id=1, source_target_pairs={{0,8},{8,0},{16,24},{24,16},{1,9},{9,1},{17,25},{25,17},{2,10},{10... | collective-permute-start | bytes 786440 | tf_op jit(solution)/shard_map/ppermute | solution.py:29
  18.8 28.5 %collective-permute-start.15 = (bf16[256,512]{1,0:T(8,128)(2,1)}, bf16[256,512]{1,0:T(8,128)(2,1)S(1)}, u32[]{:S(2)}, u32[]{:S(2)}) collective-permute-start(bf16[256,512]{1,0:T(8,128)(2,1)} %get-tuple-element.60), channel_id=1, source_target_pairs={{0,16},{8,24},{16,0},{24,8},{1,17},{9,25},{17,1},{25,9},{2,18},{10... | collective-permute-start | bytes 786440 | tf_op jit(solution)/shard_map/ppermute | solution.py:29
  28.1 23.6 %collective-permute-start.26 = (bf16[64,2048]{1,0:T(8,128)(2,1)}, bf16[64,2048]{1,0:T(8,128)(2,1)}, u32[]{:S(2)}, u32[]{:S(2)}) collective-permute-start(bf16[64,2048]{1,0:T(8,128)(2,1)} %constant_dynamic-slice_fusion.14), channel_id=1, source_target_pairs={{0,8},{8,0},{16,24},{24,16},{1,9},{9,1},{17,25},{25,17},{2,10},{10... | collective-permute-start | bytes 786440 | tf_op jit(solution)/shard_map/ppermute | solution.py:29
  28.8 43.7 %collective-permute-start = (bf16[128,2048]{1,0:T(8,128)(2,1)}, bf16[128,2048]{1,0:T(8,128)(2,1)}, u32[]{:S(2)}, u32[]{:S(2)}) collective-permute-start(bf16[128,2048]{1,0:T(8,128)(2,1)} %pad_maximum_fusion), channel_id=1, source_target_pairs={{0,16},{8,24},{16,0},{24,8},{1,17},{9,25},{17,1},{25,9},{2,18},{10... | collective-permute-start | bytes 1572872 | tf_op jit(solution)/shard_map/ppermute | solution.py:29
  41.2 24.2 %collective-permute-start.16 = (bf16[256,512]{1,0:T(8,128)(2,1)}, bf16[256,512]{1,0:T(8,128)(2,1)S(1)}, u32[]{:S(2)}, u32[]{:S(2)}) collective-permute-start(bf16[256,512]{1,0:T(8,128)(2,1)} %get-tuple-element.59), channel_id=1, source_target_pairs={{0,24},{8,16},{16,8},{24,0},{1,25},{9,17},{17,9},{25,1},{2,26},{10... | collective-permute-start | bytes 786440 | tf_op jit(solution)/shard_map/ppermute | solution.py:29
  45.8 21.8 %collective-permute-start.23 = (bf16[64,2048]{1,0:T(8,128)(2,1)S(1)}, bf16[64,2048]{1,0:T(8,128)(2,1)S(1)}, u32[]{:S(2)}, u32[]{:S(2)}) collective-permute-start(bf16[64,2048]{1,0:T(8,128)(2,1)S(1)} %collective-permute-done.22.refs_2_), channel_id=1, source_target_pairs={{0,2},{2,0},{4,6},{6,4},{1,3},{3,1},{5,7},{7,5},{8,10},{10,8},{12,... | collective-permute-start | bytes 786440 | tf_op jit(solution)/shard_map/ppermute | solution.py:29
  51.7 22.4 %collective-permute-start.27 = (bf16[64,2048]{1,0:T(8,128)(2,1)}, bf16[64,2048]{1,0:T(8,128)(2,1)S(1)}, u32[]{:S(2)}, u32[]{:S(2)}) collective-permute-start(bf16[64,2048]{1,0:T(8,128)(2,1)} %collective-permute-done.26.refs_6_), channel_id=1, source_target_pairs={{0,2},{2,0},{4,6},{6,4},{1,3},{3,1},{5,7},{7,5},{8,10},{10,8},{12,... | collective-permute-start | bytes 786440 | tf_op jit(solution)/shard_map/ppermute | solution.py:29
  72.5 22.6 %collective-permute-start.30 = (bf16[128,2048]{1,0:T(8,128)(2,1)}, bf16[128,2048]{1,0:T(8,128)(2,1)S(1)}, u32[]{:S(2)}, u32[]{:S(2)}) collective-permute-start(bf16[128,2048]{1,0:T(8,128)(2,1)} %collective-permute-done.refs_10_), channel_id=1, source_target_pairs={{0,2},{2,0},{4,6},{6,4},{1,3},{3,1},{5,7},{7,5},{8,10},{10,8},{12,... | collective-permute-start | bytes 1572872 | tf_op jit(solution)/shard_map/ppermute | solution.py:29
  75.6 20.5 %collective-permute-start.31 = (bf16[128,2048]{1,0:T(8,128)(2,1)}, bf16[128,2048]{1,0:T(8,128)(2,1)S(1)}, u32[]{:S(2)}, u32[]{:S(2)}) collective-permute-start(bf16[128,2048]{1,0:T(8,128)(2,1)} %collective-permute-done.refs_10_), channel_id=1, source_target_pairs={{0,4},{2,6},{4,0},{6,2},{1,5},{3,7},{5,1},{7,3},{8,12},{10,14},{12... | collective-permute-start | bytes 1572872 | tf_op jit(solution)/shard_map/ppermute | solution.py:29
  83.2 22.1 %collective-permute-start.1 = (bf16[128,2048]{1,0:T(8,128)(2,1)}, bf16[128,2048]{1,0:T(8,128)(2,1)S(1)}, u32[]{:S(2)}, u32[]{:S(2)}) collective-permute-start(bf16[128,2048]{1,0:T(8,128)(2,1)} %collective-permute-done.refs_10_), channel_id=1, source_target_pairs={{0,8},{8,0},{16,24},{24,16},{1,9},{9,1},{17,25},{25,17},{2,10},{10... | collective-permute-start | bytes 1572872 | tf_op jit(solution)/shard_map/ppermute | solution.py:29
  107.3 23.1 %collective-permute-start.42 = (bf16[128,2048]{1,0:T(8,128)(2,1)}, bf16[128,2048]{1,0:T(8,128)(2,1)}, u32[]{:S(2)}, u32[]{:S(2)}) collective-permute-start(bf16[128,2048]{1,0:T(8,128)(2,1)} %collective-permute-done.refs_10_), channel_id=1, source_target_pairs={{0,1},{1,0},{2,3},{3,2},{4,5},{5,4},{6,7},{7,6},{8,9},{9,8},{10,11... | collective-permute-start | bytes 1572872 | tf_op jit(solution)/shard_map/ppermute | solution.py:29
  108.4 22.2 %collective-permute-start.43 = (bf16[128,2048]{1,0:T(8,128)(2,1)S(1)}, bf16[128,2048]{1,0:T(8,128)(2,1)}, u32[]{:S(2)}, u32[]{:S(2)}) collective-permute-start(bf16[128,2048]{1,0:T(8,128)(2,1)S(1)} %collective-permute-done.30.refs_11_), channel_id=1, source_target_pairs={{0,1},{1,0},{2,3},{3,2},{4,5},{5,4},{6,7},{7,6},{8,9},{9,8},{10,11... | collective-permute-start | bytes 1572872 | tf_op jit(solution)/shard_map/ppermute | solution.py:29
  130.5 21.9 %collective-permute-start.6 = (bf16[128,2048]{1,0:T(8,128)(2,1)S(1)}, bf16[128,2048]{1,0:T(8,128)(2,1)S(1)}, u32[]{:S(2)}, u32[]{:S(2)}) collective-permute-start(bf16[128,2048]{1,0:T(8,128)(2,1)S(1)} %copy-done.5), channel_id=1, source_target_pairs={{0,1},{1,0},{2,3},{3,2},{4,5},{5,4},{6,7},{7,6},{8,9},{9,8},{10,11... | collective-permute-start | bytes 1572872 | tf_op jit(solution)/shard_map/ppermute | solution.py:29
  206.4 28.1 %collective-permute-start.59 = (bf16[512,256]{1,0:T(8,128)(2,1)S(1)}, bf16[512,256]{1,0:T(8,128)(2,1)S(1)}, u32[]{:S(2)}, u32[]{:S(2)}) collective-permute-start(bf16[512,256]{1,0:T(8,128)(2,1)S(1)} %get-tuple-element.52), channel_id=1, source_target_pairs={{0,16},{8,24},{16,0},{24,8},{1,17},{9,25},{17,1},{25,9},{2,18},{10... | collective-permute-start | bytes 786440 | tf_op jit(solution)/shard_map/ppermute | solution.py:29
  207.6 28.5 %collective-permute-start.60 = (bf16[512,256]{1,0:T(8,128)(2,1)S(1)}, bf16[512,256]{1,0:T(8,128)(2,1)S(1)}, u32[]{:S(2)}, u32[]{:S(2)}) collective-permute-start(bf16[512,256]{1,0:T(8,128)(2,1)S(1)} %get-tuple-element.51), channel_id=1, source_target_pairs={{0,24},{8,16},{16,8},{24,0},{1,25},{9,17},{17,9},{25,1},{2,26},{10... | collective-permute-start | bytes 786440 | tf_op jit(solution)/shard_map/ppermute | solution.py:29
  209.2 23.8 %collective-permute-start.53 = (bf16[64,2048]{1,0:T(8,128)(2,1)S(1)}, bf16[64,2048]{1,0:T(8,128)(2,1)S(1)}, u32[]{:S(2)}, u32[]{:S(2)}) collective-permute-start(bf16[64,2048]{1,0:T(8,128)(2,1)S(1)} %fusion.8), channel_id=1, source_target_pairs={{0,24},{8,16},{16,8},{24,0},{1,25},{9,17},{17,9},{25,1},{2,26},{10... | collective-permute-start | bytes 786440 | tf_op jit(solution)/shard_map/ppermute | solution.py:29
  213.8 22.9 %collective-permute-start.61 = (bf16[256,512]{1,0:T(8,128)(2,1)S(1)}, bf16[256,512]{1,0:T(8,128)(2,1)S(1)}, u32[]{:S(2)}, u32[]{:S(2)}) collective-permute-start(bf16[256,512]{1,0:T(8,128)(2,1)S(1)} %get-tuple-element.49), channel_id=1, source_target_pairs={{0,8},{8,0},{16,24},{24,16},{1,9},{9,1},{17,25},{25,17},{2,10},{10... | collective-permute-start | bytes 786440 | tf_op jit(solution)/shard_map/ppermute | solution.py:29
  215.8 44.8 %collective-permute-start.62 = (bf16[256,512]{1,0:T(8,128)(2,1)S(1)}, bf16[256,512]{1,0:T(8,128)(2,1)S(1)}, u32[]{:S(2)}, u32[]{:S(2)}) collective-permute-start(bf16[256,512]{1,0:T(8,128)(2,1)S(1)} %get-tuple-element.48), channel_id=1, source_target_pairs={{0,16},{8,24},{16,0},{24,8},{1,17},{9,25},{17,1},{25,9},{2,18},{10... | collective-permute-start | bytes 786440 | tf_op jit(solution)/shard_map/ppermute | solution.py:29
  232.9 27.7 %collective-permute-start.63 = (bf16[256,512]{1,0:T(8,128)(2,1)S(1)}, bf16[256,512]{1,0:T(8,128)(2,1)S(1)}, u32[]{:S(2)}, u32[]{:S(2)}) collective-permute-start(bf16[256,512]{1,0:T(8,128)(2,1)S(1)} %get-tuple-element.47), channel_id=1, source_target_pairs={{0,24},{8,16},{16,8},{24,0},{1,25},{9,17},{17,9},{25,1},{2,26},{10... | collective-permute-start | bytes 786440 | tf_op jit(solution)/shard_map/ppermute | solution.py:29
  234.5 26.6 %collective-permute-start.54 = (bf16[64,2048]{1,0:T(8,128)(2,1)S(1)}, bf16[64,2048]{1,0:T(8,128)(2,1)S(1)}, u32[]{:S(2)}, u32[]{:S(2)}) collective-permute-start(bf16[64,2048]{1,0:T(8,128)(2,1)S(1)} %get-tuple-element.42), channel_id=1, source_target_pairs={{0,2},{2,0},{4,6},{6,4},{1,3},{3,1},{5,7},{7,5},{8,10},{10,8},{12,... | collective-permute-start | bytes 786440 | tf_op jit(solution)/shard_map/ppermute | solution.py:29
  236.1 25.1 %collective-permute-start.55 = (bf16[64,2048]{1,0:T(8,128)(2,1)S(1)}, bf16[64,2048]{1,0:T(8,128)(2,1)S(1)}, u32[]{:S(2)}, u32[]{:S(2)}) collective-permute-start(bf16[64,2048]{1,0:T(8,128)(2,1)S(1)} %get-tuple-element.42), channel_id=1, source_target_pairs={{0,4},{2,6},{4,0},{6,2},{1,5},{3,7},{5,1},{7,3},{8,12},{10,14},{12... | collective-permute-start | bytes 786440 | tf_op jit(solution)/shard_map/ppermute | solution.py:29
  236.6 24.6 %collective-permute-start.56 = (bf16[64,2048]{1,0:T(8,128)(2,1)S(1)}, bf16[64,2048]{1,0:T(8,128)(2,1)S(1)}, u32[]{:S(2)}, u32[]{:S(2)}) collective-permute-start(bf16[64,2048]{1,0:T(8,128)(2,1)S(1)} %get-tuple-element.42), channel_id=1, source_target_pairs={{0,6},{2,4},{4,2},{6,0},{1,7},{3,5},{5,3},{7,1},{8,14},{10,12},{12... | collective-permute-start | bytes 786440 | tf_op jit(solution)/shard_map/ppermute | solution.py:29
  (89 other events, 675.1 us)

commit v3 on v2

--- a/solution.py
+++ b/solution.py
@@ -108,34 +108,32 @@
     )(*[mine[k] for k in whole + pieces], *[theirs[k] for k in pieces])
 
 
-def weights_kernel(w_up, w_down, *refs):
-    ups, downs, (up, down, sems) = refs[:3], refs[3:6], refs[6:]
+def weight_kernel(dim, own, *refs):
+    others, (out, sem) = refs[:3], refs[3:]
     rep = lax.axis_index("rep")
-    shard, cols = w_up.shape[0], up.shape[1]
+    shard, cols = own.shape[dim], out.shape[1 - dim]
     for j in range(4):
-        at = pl.multiple_of((rep ^ j) * shard, shard)
-        mine = pl.multiple_of(rep * cols, cols)
-        u = ups[j - 1] if j else w_up.at[:, pl.ds(mine, cols)]
-        d = downs[j - 1] if j else w_down.at[pl.ds(mine, cols), :]
-        pltpu.make_async_copy(u, up.at[pl.ds(at, shard), :], sems.at[0]).start()
-        pltpu.make_async_copy(d, down.at[:, pl.ds(at, shard)], sems.at[1]).start()
-    finish(up, sems.at[0])
-    finish(down, sems.at[1])
-
-
-def gather_weights(w_up, w_down, ups, downs):
-    (shard, cols), width = ups[0].shape, w_down.shape[1] * 4
+        at = pl.ds(pl.multiple_of((rep ^ j) * shard, shard), shard)
+        mine = pl.ds(pl.multiple_of(rep * cols, cols), cols)
+        to = out.at[at, :] if dim == 0 else out.at[:, at]
+        src = others[j - 1] if j else own.at[:, mine] if dim == 0 else own.at[mine, :]
+        pltpu.make_async_copy(src, to, sem).start()
+    finish(out, sem)
+
+
+def gather_weight(own, others, dim):
+    size = [n * 4 if d == dim else n for d, n in enumerate(others[0].shape)]
     any_space = pl.BlockSpec(memory_space=pl.ANY)
     return pl.pallas_call(
-        weights_kernel,
-        out_shape=[pltpu.VMEM((width, cols), BF16), pltpu.VMEM((cols, width), BF16)],
-        in_specs=[pl.BlockSpec(memory_space=pltpu.HBM)] * 2 + [any_space] * 6,
-        out_specs=[any_space] * 2,
-        scratch_shapes=[pltpu.SemaphoreType.DMA((2,))],
-        cost_estimate=pl.CostEstimate(flops=1_000_000_000, bytes_accessed=4 * width * cols, transcendentals=0),
+        functools.partial(weight_kernel, dim),
+        out_shape=pltpu.VMEM(tuple(size), BF16),
+        in_specs=[pl.BlockSpec(memory_space=pltpu.HBM)] + [any_space] * 3,
+        out_specs=any_space,
+        scratch_shapes=[pltpu.SemaphoreType.DMA],
+        cost_estimate=pl.CostEstimate(flops=1_000_000_000, bytes_accessed=2 * size[0] * size[1], transcendentals=0),
         compiler_params=pltpu.CompilerParams(vmem_limit_bytes=1 << 20),
-        name="weights",
-    )(w_up, w_down, *ups, *downs)
+        name="down" if dim else "up",
+    )(own, *others)
 
 
 def gathered_tokens(hidden_in, cotangent, w_up, w_down):
@@ -167,7 +165,8 @@
         ups.append(swap(u, "rep", j))
         downs.append(swap(d, "rep", j))
     near_h, at_shard = lax.optimization_barrier((near_h, at_shard))
-    up, down = gather_weights(w_up, w_down, ups, downs)
+    up = gather_weight(w_up, ups, 0)
+    down = gather_weight(w_down, downs, 1)
 
     mine = dict(hidden_in=hidden_in, cotangent=cotangent)
     theirs = {}
@@ -194,10 +193,11 @@
     def add(a, b):
         return (a.astype(F32) + b.astype(F32)).astype(BF16)
 
-    def hidden_units(hidden_rows, cot_rows):
-        active = jnp.maximum(jnp.dot(hidden_rows, up, preferred_element_type=F32), 0.0)
-        back_grad = jnp.dot(cot_rows, down.T, preferred_element_type=F32)
-        return (active * active).astype(BF16), (2.0 * active * back_grad).astype(BF16)
+    def active_units(rows):
+        return jnp.maximum(jnp.dot(rows, up, preferred_element_type=F32), 0.0)
+
+    def slopes_of(active, rows):
+        return (2.0 * active * jnp.dot(rows, down.T, preferred_element_type=F32)).astype(BF16)
 
     def between_cores(slopes):
         sent = contract_last(slopes[tokens:], up).astype(BF16)
@@ -216,9 +216,13 @@
 
     h_first, c_first = gather_rows(mine, theirs, ("near", "far"))
     h_last, c_last = gather_rows(mine, theirs, ("across", "own"))
-    hidden_first, slopes_first = hidden_units(h_first, c_first)
+    active_first = active_units(h_first)
+    active_last = active_units(h_last)
+    hidden_first = (active_first * active_first).astype(BF16)
+    hidden_last = (active_last * active_last).astype(BF16)
+    slopes_first = slopes_of(active_first, c_first)
     kept_first = between_cores(slopes_first)
-    hidden_last, slopes_last = hidden_units(h_last, c_last)
+    slopes_last = slopes_of(active_last, c_last)
     kept_last = between_cores(slopes_last)
     first = over_places(kept_first)
     last = over_places(kept_last)
@@ -244,10 +248,13 @@
             u, d = swap(u, "rep", j), swap(d, "rep", j)
         ups.append(u)
         downs.append(d)
-    ups, downs, final = lax.optimization_barrier((ups, downs, final))
+    ups[0], ups[2], ups[3], downs[0], downs[2], downs[3], final = lax.optimization_barrier(
+        (ups[0], ups[2], ups[3], downs[0], downs[2], downs[3], final)
+    )
+    ups[1], downs[1], ours = lax.optimization_barrier((ups[1], downs[1], ours))
     up_grad = jnp.zeros((shard, cols * n_rep), F32)
     down_grad = jnp.zeros((cols * n_rep, shard), F32)
-    for j in range(n_rep):
+    for j in (0, 2, 3, 1):
         up_grad = put(up_grad, ups[j].astype(F32), at_cols[j], 1)
         down_grad = put(down_grad, downs[j].astype(F32), at_cols[j], 0)
     return input_grad, up_grad, down_grad

time: 270 us -> 262 us (0.970); the launches traced: 265 us -> 261 us
  local copies, waits for them, and re-layouts: 46.9 us -> 33.6 us
  starting transfers between devices: 81.9 us -> 91.3 us
    unnamed x102, local copies, waits for them, and re-layouts: 36.4 us -> 23.8 us
    ppermute x64, starting transfers between devices: 81.9 us -> 91.3 us  [swap(): return lax.ppermute(value, axis, [(i, i ^ offset) for i in range(size)])]
  transfers between devices with their start and end apart: 64 -> 64, of which waited for: 20 -> 23; matrix products, arithmetic and copies ran while one was open for 10% -> 9% of each run, Pallas kernels for 1% -> 1%
where the time goes in v3:
time: 262 us; the launch traced here: 261 us
  waiting for transfers between devices  115 us (44%)
  starting transfers between devices  91.3 us (35%)
  local copies, waits for them, and re-layouts  33.6 us (13%)
  matrix products  13.6 us (5%)
  Pallas kernels  3.63 us (1%)
    ppermute x64, waiting for transfers between devices, swap(): return lax.ppermute(value, axis, [(i, i ^ offset) for i in range(size)])  115 us
    ppermute x64, starting transfers between devices, swap(): return lax.ppermute(value, axis, [(i, i ^ offset) for i in range(size)])  91.3 us
    unnamed x102, local copies, waits for them, and re-layouts  23.8 us
    dynamic_slice x6, local copies, waits for them, and re-layouts, cut(): return lax.dynamic_slice(value, starts, sizes, allow_negative_indices=False)  5.73 us
    dot_general x4, matrix products, contract_first(): lax.dot_general(left, right, (((0,), (0,)), ((), ())), preferred_element_...  5.54 us
  transfers between devices with their start and end apart: 64, of which 23 were waited for; matrix products, arithmetic and copies ran while one was open for 9% of the time, Pallas kernels for 1%

profile of v3, /device:TPU:0, one launch (start us, length us, event | category | flops | bytes accessed | tf_op | source)
XLA Modules:
  0.0 261.2 jit_solution(12248903860512788083)
XLA Ops:
  2.8 3.1 %collective-permute-start.11 = (bf16[512,256]{1,0:T(8,128)(2,1)}, bf16[512,256]{1,0:T(8,128)(2,1)S(1)}, u32[]{:S(2)}, u32[]{:S(2)}) collective-permute-start(bf16[512,256]{1,0:T(8,128)(2,1)} %get-tuple-element.60), channel_id=1, source_target_pairs={{0,8},{8,0},{16,24},{24,16},{1,9},{9,1},{17,25},{25,17},{2,10},{10... | collective-permute-start | bytes 786440 | tf_op jit(solution)/shard_map/ppermute | solution.py:29
  5.8 2.6 collective-permute-start.12
  14.2 3.8 %collective-permute-done.11.refs_0_ = bf16[512,256]{1,0:T(8,128)(2,1)S(1)} collective-permute-done((bf16[512,256]{1,0:T(8,128)(2,1)}, bf16[512,256]{1,0:T(8,128)(2,1)S(1)}, u32[]{:S(2)}, u32[]{:S(2)}) %collective-permute-start.11) | collective-permute-done | bytes 262176 | tf_op jit(solution)/shard_map/ppermute | solution.py:29
  18.8 8.6 %collective-permute-done.12.refs_1_ = bf16[512,256]{1,0:T(8,128)(2,1)S(1)} collective-permute-done((bf16[512,256]{1,0:T(8,128)(2,1)}, bf16[512,256]{1,0:T(8,128)(2,1)S(1)}, u32[]{:S(2)}, u32[]{:S(2)}) %collective-permute-start.12) | collective-permute-done | bytes 262176 | tf_op jit(solution)/shard_map/ppermute | solution.py:29
  28.8 6.5 %collective-permute-start.15 = (bf16[256,512]{1,0:T(8,128)(2,1)}, bf16[256,512]{1,0:T(8,128)(2,1)S(1)}, u32[]{:S(2)}, u32[]{:S(2)}) collective-permute-start(bf16[256,512]{1,0:T(8,128)(2,1)} %get-tuple-element.56), channel_id=1, source_target_pairs={{0,16},{8,24},{16,0},{24,8},{1,17},{9,25},{17,1},{25,9},{2,18},{10... | collective-permute-start | bytes 786440 | tf_op jit(solution)/shard_map/ppermute | solution.py:29
  36.6 10.3 %collective-permute-done.26.refs_6_ = bf16[64,2048]{1,0:T(8,128)(2,1)} collective-permute-done((bf16[64,2048]{1,0:T(8,128)(2,1)S(1)}, bf16[64,2048]{1,0:T(8,128)(2,1)}, u32[]{:S(2)}, u32[]{:S(2)}) %collective-permute-start.26) | collective-permute-done | bytes 262176 | tf_op jit(solution)/shard_map/ppermute | solution.py:29
  48.8 2.7 %collective-permute-done.14.refs_0_ = bf16[256,512]{1,0:T(8,128)(2,1)S(1)} collective-permute-done((bf16[256,512]{1,0:T(8,128)(2,1)}, bf16[256,512]{1,0:T(8,128)(2,1)S(1)}, u32[]{:S(2)}, u32[]{:S(2)}) %collective-permute-start.14) | collective-permute-done | bytes 262176 | tf_op jit(solution)/shard_map/ppermute | solution.py:29
  53.9 18.4 %collective-permute-done.15.refs_1_ = bf16[256,512]{1,0:T(8,128)(2,1)S(1)} collective-permute-done((bf16[256,512]{1,0:T(8,128)(2,1)}, bf16[256,512]{1,0:T(8,128)(2,1)S(1)}, u32[]{:S(2)}, u32[]{:S(2)}) %collective-permute-start.15) | collective-permute-done | bytes 262176 | tf_op jit(solution)/shard_map/ppermute | solution.py:29
  83.6 2.4 collective-permute-start.31
  89.1 3.3 %collective-permute-start.1 = (bf16[128,2048]{1,0:T(8,128)(2,1)}, bf16[128,2048]{1,0:T(8,128)(2,1)S(1)}, u32[]{:S(2)}, u32[]{:S(2)}) collective-permute-start(bf16[128,2048]{1,0:T(8,128)(2,1)} %collective-permute-done.refs_10_), channel_id=1, source_target_pairs={{0,8},{8,0},{16,24},{24,16},{1,9},{9,1},{17,25},{25,17},{2,10},{10... | collective-permute-start | bytes 1572872 | tf_op jit(solution)/shard_map/ppermute | solution.py:29
  92.4 4.6 %collective-permute-done.29.refs_9_ = bf16[64,2048]{1,0:T(8,128)(2,1)S(1)} collective-permute-done((bf16[64,2048]{1,0:T(8,128)(2,1)S(1)}, bf16[64,2048]{1,0:T(8,128)(2,1)S(1)}, u32[]{:S(2)}, u32[]{:S(2)}) %collective-permute-start.29) | collective-permute-done | bytes 262176 | tf_op jit(solution)/shard_map/ppermute | solution.py:29
  110.0 3.1 %collective-permute-done.32.refs_13_ = bf16[64,2048]{1,0:T(8,128)(2,1)} collective-permute-done((bf16[64,2048]{1,0:T(8,128)(2,1)S(1)}, bf16[64,2048]{1,0:T(8,128)(2,1)}, u32[]{:S(2)}, u32[]{:S(2)}) %collective-permute-start.32) | collective-permute-done | bytes 262176 | tf_op jit(solution)/shard_map/ppermute | solution.py:29
  114.8 10.5 %collective-permute-done.2.refs_3_ = bf16[128,2048]{1,0:T(8,128)(2,1)} collective-permute-done((bf16[128,2048]{1,0:T(8,128)(2,1)S(1)}, bf16[128,2048]{1,0:T(8,128)(2,1)}, u32[]{:S(2)}, u32[]{:S(2)}) %collective-permute-start.2) | collective-permute-done | bytes 524320 | tf_op jit(solution)/shard_map/ppermute | solution.py:29
  156.7 10.6 %collective-permute-done.50 = bf16[2,2,64,1024]{3,2,0,1:T(8,128)(2,1)S(1)} collective-permute-done((bf16[2,2,64,1024]{3,2,0,1:T(8,128)(2,1)S(1)}, bf16[2,2,64,1024]{3,2,0,1:T(8,128)(2,1)S(1)}, u32[]{:S(2)}, u32[]{:S(2)}) %collective-permute-start.50) | collective-permute-done | bytes 524320 | tf_op jit(solution)/shard_map/ppermute | solution.py:29
  173.2 3.5 %collective-permute-done.51 = bf16[2,64,1024]{2,1,0:T(8,128)(2,1)S(1)} collective-permute-done((bf16[2,64,1024]{2,1,0:T(8,128)(2,1)S(1)}, bf16[2,64,1024]{2,1,0:T(8,128)(2,1)S(1)}, u32[]{:S(2)}, u32[]{:S(2)}) %collective-permute-start.51) | collective-permute-done | bytes 262176 | tf_op jit(solution)/shard_map/ppermute | solution.py:29
  176.8 3.1 %collective-permute-done.49 = bf16[2,64,1024]{2,1,0:T(8,128)(2,1)S(1)} collective-permute-done((bf16[2,64,1024]{2,1,0:T(8,128)(2,1)S(1)}, bf16[2,64,1024]{2,1,0:T(8,128)(2,1)S(1)}, u32[]{:S(2)}, u32[]{:S(2)}) %collective-permute-start.49) | collective-permute-done | bytes 262176 | tf_op jit(solution)/shard_map/ppermute | solution.py:29
  181.9 7.1 %collective-permute-done.20 = bf16[2,2,64,1024]{3,2,0,1:T(8,128)(2,1)S(1)} collective-permute-done((bf16[2,2,64,1024]{3,2,0,1:T(8,128)(2,1)S(1)}, bf16[2,2,64,1024]{3,2,0,1:T(8,128)(2,1)S(1)}, u32[]{:S(2)}, u32[]{:S(2)}) %collective-permute-start.20) | collective-permute-done | bytes 524320 | tf_op jit(solution)/shard_map/ppermute | solution.py:29
  191.9 3.3 %collective-permute-start.58 = (bf16[512,256]{1,0:T(8,128)(2,1)S(1)}, bf16[512,256]{1,0:T(8,128)(2,1)S(1)}, u32[]{:S(2)}, u32[]{:S(2)}) collective-permute-start(bf16[512,256]{1,0:T(8,128)(2,1)S(1)} %get-tuple-element.49), channel_id=1, source_target_pairs={{0,16},{8,24},{16,0},{24,8},{1,17},{9,25},{17,1},{25,9},{2,18},{10... | collective-permute-start | bytes 786440 | tf_op jit(solution)/shard_map/ppermute | solution.py:29
  196.8 2.5 collective-permute-start.53
  203.5 2.5 collective-permute-start.61
  205.9 9.1 %collective-permute-done.53 = bf16[64,2048]{1,0:T(8,128)(2,1)S(1)} collective-permute-done((bf16[64,2048]{1,0:T(8,128)(2,1)S(1)}, bf16[64,2048]{1,0:T(8,128)(2,1)S(1)}, u32[]{:S(2)}, u32[]{:S(2)}) %collective-permute-start.53) | collective-permute-done | bytes 262176 | tf_op jit(solution)/shard_map/ppermute | solution.py:29
  215.0 25.3 %collective-permute-start.62 = (bf16[512,256]{1,0:T(8,128)(2,1)S(1)}, bf16[512,256]{1,0:T(8,128)(2,1)S(1)}, u32[]{:S(2)}, u32[]{:S(2)}) collective-permute-start(bf16[512,256]{1,0:T(8,128)(2,1)S(1)} %get-tuple-element.47), channel_id=1, source_target_pairs={{0,8},{8,0},{16,24},{24,16},{1,9},{9,1},{17,25},{25,17},{2,10},{10... | collective-permute-start | bytes 786440 | tf_op jit(solution)/shard_map/ppermute | solution.py:29
  242.1 3.3 %collective-permute-done.60 = bf16[256,512]{1,0:T(8,128)(2,1)S(1)} collective-permute-done((bf16[256,512]{1,0:T(8,128)(2,1)S(1)}, bf16[256,512]{1,0:T(8,128)(2,1)S(1)}, u32[]{:S(2)}, u32[]{:S(2)}) %collective-permute-start.60) | collective-permute-done | bytes 262176 | tf_op jit(solution)/shard_map/ppermute | solution.py:29
  249.0 8.0 %collective-permute-done.55 = bf16[64,2048]{1,0:T(8,128)(2,1)S(1)} collective-permute-done((bf16[64,2048]{1,0:T(8,128)(2,1)S(1)}, bf16[64,2048]{1,0:T(8,128)(2,1)S(1)}, u32[]{:S(2)}, u32[]{:S(2)}) %collective-permute-start.55) | collective-permute-done | bytes 262176 | tf_op jit(solution)/shard_map/ppermute | solution.py:29
  (271 shorter events, 101.5 us)
Async XLA Ops:
  5.8 21.6 %collective-permute-start.12 = (bf16[512,256]{1,0:T(8,128)(2,1)}, bf16[512,256]{1,0:T(8,128)(2,1)S(1)}, u32[]{:S(2)}, u32[]{:S(2)}) collective-permute-start(bf16[512,256]{1,0:T(8,128)(2,1)} %get-tuple-element.59), channel_id=1, source_target_pairs={{0,16},{8,24},{16,0},{24,8},{1,17},{9,25},{17,1},{25,9},{2,18},{10... | collective-permute-start | bytes 786440 | tf_op jit(solution)/shard_map/ppermute | solution.py:29
  8.4 19.7 %collective-permute-start.13 = (bf16[512,256]{1,0:T(8,128)(2,1)}, bf16[512,256]{1,0:T(8,128)(2,1)S(1)}, u32[]{:S(2)}, u32[]{:S(2)}) collective-permute-start(bf16[512,256]{1,0:T(8,128)(2,1)} %get-tuple-element.58), channel_id=1, source_target_pairs={{0,24},{8,16},{16,8},{24,0},{1,25},{9,17},{17,9},{25,1},{2,26},{10... | collective-permute-start | bytes 786440 | tf_op jit(solution)/shard_map/ppermute | solution.py:29
  9.4 25.9 %collective-permute-start.22 = (bf16[64,2048]{1,0:T(8,128)(2,1)S(1)}, bf16[64,2048]{1,0:T(8,128)(2,1)S(1)}, u32[]{:S(2)}, u32[]{:S(2)}) collective-permute-start(bf16[64,2048]{1,0:T(8,128)(2,1)S(1)} %constant_dynamic-slice_fusion.15), channel_id=1, source_target_pairs={{0,8},{8,0},{16,24},{24,16},{1,9},{9,1},{17,25},{25,17},{2,10},{10... | collective-permute-start | bytes 786440 | tf_op jit(solution)/shard_map/ppermute | solution.py:29
  11.3 35.6 %collective-permute-start.26 = (bf16[64,2048]{1,0:T(8,128)(2,1)S(1)}, bf16[64,2048]{1,0:T(8,128)(2,1)}, u32[]{:S(2)}, u32[]{:S(2)}) collective-permute-start(bf16[64,2048]{1,0:T(8,128)(2,1)S(1)} %constant_dynamic-slice_fusion.14), channel_id=1, source_target_pairs={{0,8},{8,0},{16,24},{24,16},{1,9},{9,1},{17,25},{25,17},{2,10},{10... | collective-permute-start | bytes 786440 | tf_op jit(solution)/shard_map/ppermute | solution.py:29
  18.8 32.8 %collective-permute-start.14 = (bf16[256,512]{1,0:T(8,128)(2,1)}, bf16[256,512]{1,0:T(8,128)(2,1)S(1)}, u32[]{:S(2)}, u32[]{:S(2)}) collective-permute-start(bf16[256,512]{1,0:T(8,128)(2,1)} %get-tuple-element.57), channel_id=1, source_target_pairs={{0,8},{8,0},{16,24},{24,16},{1,9},{9,1},{17,25},{25,17},{2,10},{10... | collective-permute-start | bytes 786440 | tf_op jit(solution)/shard_map/ppermute | solution.py:29
  28.1 49.2 %collective-permute-start = (bf16[128,2048]{1,0:T(8,128)(2,1)}, bf16[128,2048]{1,0:T(8,128)(2,1)}, u32[]{:S(2)}, u32[]{:S(2)}) collective-permute-start(bf16[128,2048]{1,0:T(8,128)(2,1)} %pad_maximum_fusion), channel_id=1, source_target_pairs={{0,16},{8,24},{16,0},{24,8},{1,17},{9,25},{17,1},{25,9},{2,18},{10... | collective-permute-start | bytes 1572872 | tf_op jit(solution)/shard_map/ppermute | solution.py:29
  28.8 43.6 %collective-permute-start.15 = (bf16[256,512]{1,0:T(8,128)(2,1)}, bf16[256,512]{1,0:T(8,128)(2,1)S(1)}, u32[]{:S(2)}, u32[]{:S(2)}) collective-permute-start(bf16[256,512]{1,0:T(8,128)(2,1)} %get-tuple-element.56), channel_id=1, source_target_pairs={{0,16},{8,24},{16,0},{24,8},{1,17},{9,25},{17,1},{25,9},{2,18},{10... | collective-permute-start | bytes 786440 | tf_op jit(solution)/shard_map/ppermute | solution.py:29
  35.3 39.3 %collective-permute-start.16 = (bf16[256,512]{1,0:T(8,128)(2,1)}, bf16[256,512]{1,0:T(8,128)(2,1)S(1)}, u32[]{:S(2)}, u32[]{:S(2)}) collective-permute-start(bf16[256,512]{1,0:T(8,128)(2,1)} %get-tuple-element.55), channel_id=1, source_target_pairs={{0,24},{8,16},{16,8},{24,0},{1,25},{9,17},{17,9},{25,1},{2,26},{10... | collective-permute-start | bytes 786440 | tf_op jit(solution)/shard_map/ppermute | solution.py:29
  46.9 29.9 %collective-permute-start.23 = (bf16[64,2048]{1,0:T(8,128)(2,1)S(1)}, bf16[64,2048]{1,0:T(8,128)(2,1)S(1)}, u32[]{:S(2)}, u32[]{:S(2)}) collective-permute-start(bf16[64,2048]{1,0:T(8,128)(2,1)S(1)} %collective-permute-done.22.refs_2_), channel_id=1, source_target_pairs={{0,2},{2,0},{4,6},{6,4},{1,3},{3,1},{5,7},{7,5},{8,10},{10,8},{12,... | collective-permute-start | bytes 786440 | tf_op jit(solution)/shard_map/ppermute | solution.py:29
  52.2 24.6 %collective-permute-start.24 = (bf16[64,2048]{1,0:T(8,128)(2,1)S(1)}, bf16[64,2048]{1,0:T(8,128)(2,1)S(1)}, u32[]{:S(2)}, u32[]{:S(2)}) collective-permute-start(bf16[64,2048]{1,0:T(8,128)(2,1)S(1)} %collective-permute-done.22.refs_2_), channel_id=1, source_target_pairs={{0,4},{2,6},{4,0},{6,2},{1,5},{3,7},{5,1},{7,3},{8,12},{10,14},{12... | collective-permute-start | bytes 786440 | tf_op jit(solution)/shard_map/ppermute | solution.py:29
  77.3 22.3 %collective-permute-start.30 = (bf16[128,2048]{1,0:T(8,128)(2,1)}, bf16[128,2048]{1,0:T(8,128)(2,1)S(1)}, u32[]{:S(2)}, u32[]{:S(2)}) collective-permute-start(bf16[128,2048]{1,0:T(8,128)(2,1)} %collective-permute-done.refs_10_), channel_id=1, source_target_pairs={{0,2},{2,0},{4,6},{6,4},{1,3},{3,1},{5,7},{7,5},{8,10},{10,8},{12,... | collective-permute-start | bytes 1572872 | tf_op jit(solution)/shard_map/ppermute | solution.py:29
  89.1 17.8 %collective-permute-start.1 = (bf16[128,2048]{1,0:T(8,128)(2,1)}, bf16[128,2048]{1,0:T(8,128)(2,1)S(1)}, u32[]{:S(2)}, u32[]{:S(2)}) collective-permute-start(bf16[128,2048]{1,0:T(8,128)(2,1)} %collective-permute-done.refs_10_), channel_id=1, source_target_pairs={{0,8},{8,0},{16,24},{24,16},{1,9},{9,1},{17,25},{25,17},{2,10},{10... | collective-permute-start | bytes 1572872 | tf_op jit(solution)/shard_map/ppermute | solution.py:29
  107.0 18.3 %collective-permute-start.2 = (bf16[128,2048]{1,0:T(8,128)(2,1)S(1)}, bf16[128,2048]{1,0:T(8,128)(2,1)}, u32[]{:S(2)}, u32[]{:S(2)}) collective-permute-start(bf16[128,2048]{1,0:T(8,128)(2,1)S(1)} %collective-permute-done.1.refs_2_), channel_id=1, source_target_pairs={{0,2},{2,0},{4,6},{6,4},{1,3},{3,1},{5,7},{7,5},{8,10},{10,8},{12,... | collective-permute-start | bytes 1572872 | tf_op jit(solution)/shard_map/ppermute | solution.py:29
  110.0 22.2 %collective-permute-start.42 = (bf16[128,2048]{1,0:T(8,128)(2,1)}, bf16[128,2048]{1,0:T(8,128)(2,1)}, u32[]{:S(2)}, u32[]{:S(2)}) collective-permute-start(bf16[128,2048]{1,0:T(8,128)(2,1)} %collective-permute-done.refs_10_), channel_id=1, source_target_pairs={{0,1},{1,0},{2,3},{3,2},{4,5},{5,4},{6,7},{7,6},{8,9},{9,8},{10,11... | collective-permute-start | bytes 1572872 | tf_op jit(solution)/shard_map/ppermute | solution.py:29
  113.1 19.2 %collective-permute-start.43 = (bf16[128,2048]{1,0:T(8,128)(2,1)S(1)}, bf16[128,2048]{1,0:T(8,128)(2,1)}, u32[]{:S(2)}, u32[]{:S(2)}) collective-permute-start(bf16[128,2048]{1,0:T(8,128)(2,1)S(1)} %collective-permute-done.30.refs_11_), channel_id=1, source_target_pairs={{0,1},{1,0},{2,3},{3,2},{4,5},{5,4},{6,7},{7,6},{8,9},{9,8},{10,11... | collective-permute-start | bytes 1572872 | tf_op jit(solution)/shard_map/ppermute | solution.py:29
  114.8 18.6 %collective-permute-start.44 = (bf16[128,2048]{1,0:T(8,128)(2,1)S(1)}, bf16[128,2048]{1,0:T(8,128)(2,1)}, u32[]{:S(2)}, u32[]{:S(2)}) collective-permute-start(bf16[128,2048]{1,0:T(8,128)(2,1)S(1)} %collective-permute-done.31.refs_12_), channel_id=1, source_target_pairs={{0,1},{1,0},{2,3},{3,2},{4,5},{5,4},{6,7},{7,6},{8,9},{9,8},{10,11... | collective-permute-start | bytes 1572872 | tf_op jit(solution)/shard_map/ppermute | solution.py:29
  149.1 19.6 %collective-permute-start.17 = (bf16[512,2048]{1,0:T(8,128)(2,1)S(1)}, bf16[512,2048]{1,0:T(8,128)(2,1)S(1)}, u32[]{:S(2)}, u32[]{:S(2)}) collective-permute-start(bf16[512,2048]{1,0:T(8,128)(2,1)S(1)} %convolution_convert_fusion.1), channel_id=1, source_target_pairs={{0,1},{1,0},{2,3},{3,2},{4,5},{5,4},{6,7},{7,6},{8,9},{9,8},{10,11... | collective-permute-start | bytes 6291464 | tf_op jit(solution)/shard_map/ppermute | solution.py:29
  170.9 18.1 %collective-permute-start.20 = (bf16[2,2,64,1024]{3,2,0,1:T(8,128)(2,1)S(1)}, bf16[2,2,64,1024]{3,2,0,1:T(8,128)(2,1)S(1)}, u32[]{:S(2)}, u32[]{:S(2)}) collective-permute-start(bf16[2,2,64,1024]{3,2,0,1:T(8,128)(2,1)S(1)} %copy.17), channel_id=1, source_target_pairs={{0,4},{2,6},{4,0},{6,2},{1,5},{3,7},{5,1},{7,3},{8,12},{10,14},{12... | collective-permute-start | bytes 1572872 | tf_op jit(solution)/shard_map/ppermute | solution.py:29
  191.9 48.7 %collective-permute-start.58 = (bf16[512,256]{1,0:T(8,128)(2,1)S(1)}, bf16[512,256]{1,0:T(8,128)(2,1)S(1)}, u32[]{:S(2)}, u32[]{:S(2)}) collective-permute-start(bf16[512,256]{1,0:T(8,128)(2,1)S(1)} %get-tuple-element.49), channel_id=1, source_target_pairs={{0,16},{8,24},{16,0},{24,8},{1,17},{9,25},{17,1},{25,9},{2,18},{10... | collective-permute-start | bytes 786440 | tf_op jit(solution)/shard_map/ppermute | solution.py:29
  195.2 45.4 %collective-permute-start.59 = (bf16[512,256]{1,0:T(8,128)(2,1)S(1)}, bf16[512,256]{1,0:T(8,128)(2,1)S(1)}, u32[]{:S(2)}, u32[]{:S(2)}) collective-permute-start(bf16[512,256]{1,0:T(8,128)(2,1)S(1)} %get-tuple-element.48), channel_id=1, source_target_pairs={{0,24},{8,16},{16,8},{24,0},{1,25},{9,17},{17,9},{25,1},{2,26},{10... | collective-permute-start | bytes 786440 | tf_op jit(solution)/shard_map/ppermute | solution.py:29
  196.8 18.2 %collective-permute-start.53 = (bf16[64,2048]{1,0:T(8,128)(2,1)S(1)}, bf16[64,2048]{1,0:T(8,128)(2,1)S(1)}, u32[]{:S(2)}, u32[]{:S(2)}) collective-permute-start(bf16[64,2048]{1,0:T(8,128)(2,1)S(1)} %fusion.8), channel_id=1, source_target_pairs={{0,24},{8,16},{16,8},{24,0},{1,25},{9,17},{17,9},{25,1},{2,26},{10... | collective-permute-start | bytes 786440 | tf_op jit(solution)/shard_map/ppermute | solution.py:29
  201.4 44.0 %collective-permute-start.60 = (bf16[256,512]{1,0:T(8,128)(2,1)S(1)}, bf16[256,512]{1,0:T(8,128)(2,1)S(1)}, u32[]{:S(2)}, u32[]{:S(2)}) collective-permute-start(bf16[256,512]{1,0:T(8,128)(2,1)S(1)} %get-tuple-element.45), channel_id=1, source_target_pairs={{0,16},{8,24},{16,0},{24,8},{1,17},{9,25},{17,1},{25,9},{2,18},{10... | collective-permute-start | bytes 786440 | tf_op jit(solution)/shard_map/ppermute | solution.py:29
  203.5 43.7 %collective-permute-start.61 = (bf16[256,512]{1,0:T(8,128)(2,1)S(1)}, bf16[256,512]{1,0:T(8,128)(2,1)S(1)}, u32[]{:S(2)}, u32[]{:S(2)}) collective-permute-start(bf16[256,512]{1,0:T(8,128)(2,1)S(1)} %get-tuple-element.44), channel_id=1, source_target_pairs={{0,24},{8,16},{16,8},{24,0},{1,25},{9,17},{17,9},{25,1},{2,26},{10... | collective-permute-start | bytes 786440 | tf_op jit(solution)/shard_map/ppermute | solution.py:29
  215.0 42.3 %collective-permute-start.62 = (bf16[512,256]{1,0:T(8,128)(2,1)S(1)}, bf16[512,256]{1,0:T(8,128)(2,1)S(1)}, u32[]{:S(2)}, u32[]{:S(2)}) collective-permute-start(bf16[512,256]{1,0:T(8,128)(2,1)S(1)} %get-tuple-element.47), channel_id=1, source_target_pairs={{0,8},{8,0},{16,24},{24,16},{1,9},{9,1},{17,25},{25,17},{2,10},{10... | collective-permute-start | bytes 786440 | tf_op jit(solution)/shard_map/ppermute | solution.py:29
  (89 other events, 628.2 us)

commit v4 on v3

--- a/solution.py
+++ b/solution.py
@@ -226,9 +226,8 @@
     kept_last = between_cores(slopes_last)
     first = over_places(kept_first)
     last = over_places(kept_last)
-    got = swap(first, "rep", 1)
-    own_sum = last[1].astype(F32) + got[0].astype(F32)
-    across_sum = add(last[0], got[1])
+    across_sum = add(last[0], swap(first[1], "rep", 1))
+    own_sum = last[1].astype(F32) + swap(first[0], "rep", 1).astype(F32)
     final = (own_sum + swap(across_sum, "rep", 3).astype(F32)).astype(BF16)
     blocks = [final] + [swap(final, "fs", b) for b in (1, 2, 3)]
     ours = jnp.zeros((side, width), BF16)
@@ -248,13 +247,12 @@
             u, d = swap(u, "rep", j), swap(d, "rep", j)
         ups.append(u)
         downs.append(d)
-    ups[0], ups[2], ups[3], downs[0], downs[2], downs[3], final = lax.optimization_barrier(
-        (ups[0], ups[2], ups[3], downs[0], downs[2], downs[3], final)
-    )
-    ups[1], downs[1], ours = lax.optimization_barrier((ups[1], downs[1], ours))
+    early = (ups[:3], downs, final)
+    (ups[0], ups[1], ups[2]), downs, final = lax.optimization_barrier(early)
+    ups[3], ours = lax.optimization_barrier((ups[3], ours))
     up_grad = jnp.zeros((shard, cols * n_rep), F32)
     down_grad = jnp.zeros((cols * n_rep, shard), F32)
-    for j in (0, 2, 3, 1):
+    for j in range(n_rep):
         up_grad = put(up_grad, ups[j].astype(F32), at_cols[j], 1)
         down_grad = put(down_grad, downs[j].astype(F32), at_cols[j], 0)
     return input_grad, up_grad, down_grad

time: 262 us -> 253 us (0.966)
  starting transfers between devices: 91.3 us -> 62 us
  waiting for transfers between devices: 115 us -> 136 us
    ppermute x64 -> x65, starting transfers between devices: 91.3 us -> 62 us  [swap(): return lax.ppermute(value, axis, [(i, i ^ offset) for i in range(size)])]
    ppermute x64 -> x65, waiting for transfers between devices: 115 us -> 136 us  [swap(): return lax.ppermute(value, axis, [(i, i ^ offset) for i in range(size)])]
  transfers between devices with their start and end apart: 64 -> 65, of which waited for: 23 -> 25; matrix products, arithmetic and copies ran while one was open for 9% -> 9% of each run, Pallas kernels for 1% -> 1%
where the time goes in v4:
time: 253 us; the launch traced here: 252 us
  waiting for transfers between devices  136 us (54%)
  starting transfers between devices  62 us (25%)
  local copies, waits for them, and re-layouts  33.6 us (13%)
  matrix products  13.6 us (5%)
  Pallas kernels  3.63 us (1%)
    ppermute x65, waiting for transfers between devices, swap(): return lax.ppermute(value, axis, [(i, i ^ offset) for i in range(size)])  136 us
    ppermute x65, starting transfers between devices, swap(): return lax.ppermute(value, axis, [(i, i ^ offset) for i in range(size)])  62 us
    unnamed x102, local copies, waits for them, and re-layouts  23.8 us
    dynamic_slice x6, local copies, waits for them, and re-layouts, cut(): return lax.dynamic_slice(value, starts, sizes, allow_negative_indices=False)  5.78 us
    dot_general x4, matrix products, contract_first(): lax.dot_general(left, right, (((0,), (0,)), ((), ())), preferred_element_...  5.55 us
  transfers between devices with their start and end apart: 65, of which 25 were waited for; matrix products, arithmetic and copies ran while one was open for 9% of the time, Pallas kernels for 1%

profile of v4, /device:TPU:0, one launch (start us, length us, event | category | flops | bytes accessed | tf_op | source)
XLA Modules:
  0.0 252.5 jit_solution(4460790914591483685)
XLA Ops:
  0.7 2.1 constant_dynamic-slice_fusion.11
  2.8 3.1 %collective-permute-start.11 = (bf16[512,256]{1,0:T(8,128)(2,1)}, bf16[512,256]{1,0:T(8,128)(2,1)S(1)}, u32[]{:S(2)}, u32[]{:S(2)}) collective-permute-start(bf16[512,256]{1,0:T(8,128)(2,1)} %get-tuple-element.60), channel_id=1, source_target_pairs={{0,8},{8,0},{16,24},{24,16},{1,9},{9,1},{17,25},{25,17},{2,10},{10... | collective-permute-start | bytes 786440 | tf_op jit(solution)/shard_map/ppermute | solution.py:29
  5.8 2.6 %collective-permute-start.12 = (bf16[512,256]{1,0:T(8,128)(2,1)}, bf16[512,256]{1,0:T(8,128)(2,1)S(1)}, u32[]{:S(2)}, u32[]{:S(2)}) collective-permute-start(bf16[512,256]{1,0:T(8,128)(2,1)} %get-tuple-element.59), channel_id=1, source_target_pairs={{0,16},{8,24},{16,0},{24,8},{1,17},{9,25},{17,1},{25,9},{2,18},{10... | collective-permute-start | bytes 786440 | tf_op jit(solution)/shard_map/ppermute | solution.py:29
  14.3 3.8 %collective-permute-done.11.refs_0_ = bf16[512,256]{1,0:T(8,128)(2,1)S(1)} collective-permute-done((bf16[512,256]{1,0:T(8,128)(2,1)}, bf16[512,256]{1,0:T(8,128)(2,1)S(1)}, u32[]{:S(2)}, u32[]{:S(2)}) %collective-permute-start.11) | collective-permute-done | bytes 262176 | tf_op jit(solution)/shard_map/ppermute | solution.py:29
  18.8 8.6 %collective-permute-done.12.refs_1_ = bf16[512,256]{1,0:T(8,128)(2,1)S(1)} collective-permute-done((bf16[512,256]{1,0:T(8,128)(2,1)}, bf16[512,256]{1,0:T(8,128)(2,1)S(1)}, u32[]{:S(2)}, u32[]{:S(2)}) %collective-permute-start.12) | collective-permute-done | bytes 262176 | tf_op jit(solution)/shard_map/ppermute | solution.py:29
  28.8 6.5 %collective-permute-start.15 = (bf16[256,512]{1,0:T(8,128)(2,1)}, bf16[256,512]{1,0:T(8,128)(2,1)S(1)}, u32[]{:S(2)}, u32[]{:S(2)}) collective-permute-start(bf16[256,512]{1,0:T(8,128)(2,1)} %get-tuple-element.56), channel_id=1, source_target_pairs={{0,16},{8,24},{16,0},{24,8},{1,17},{9,25},{17,1},{25,9},{2,18},{10... | collective-permute-start | bytes 786440 | tf_op jit(solution)/shard_map/ppermute | solution.py:29
  36.6 10.3 %collective-permute-done.26.refs_6_ = bf16[64,2048]{1,0:T(8,128)(2,1)} collective-permute-done((bf16[64,2048]{1,0:T(8,128)(2,1)S(1)}, bf16[64,2048]{1,0:T(8,128)(2,1)}, u32[]{:S(2)}, u32[]{:S(2)}) %collective-permute-start.26) | collective-permute-done | bytes 262176 | tf_op jit(solution)/shard_map/ppermute | solution.py:29
  48.8 2.7 %collective-permute-done.14.refs_0_ = bf16[256,512]{1,0:T(8,128)(2,1)S(1)} collective-permute-done((bf16[256,512]{1,0:T(8,128)(2,1)}, bf16[256,512]{1,0:T(8,128)(2,1)S(1)}, u32[]{:S(2)}, u32[]{:S(2)}) %collective-permute-start.14) | collective-permute-done | bytes 262176 | tf_op jit(solution)/shard_map/ppermute | solution.py:29
  53.9 18.4 %collective-permute-done.15.refs_1_ = bf16[256,512]{1,0:T(8,128)(2,1)S(1)} collective-permute-done((bf16[256,512]{1,0:T(8,128)(2,1)}, bf16[256,512]{1,0:T(8,128)(2,1)S(1)}, u32[]{:S(2)}, u32[]{:S(2)}) %collective-permute-start.15) | collective-permute-done | bytes 262176 | tf_op jit(solution)/shard_map/ppermute | solution.py:29
  83.6 2.4 collective-permute-start.31
  89.1 3.3 %collective-permute-start.1 = (bf16[128,2048]{1,0:T(8,128)(2,1)}, bf16[128,2048]{1,0:T(8,128)(2,1)S(1)}, u32[]{:S(2)}, u32[]{:S(2)}) collective-permute-start(bf16[128,2048]{1,0:T(8,128)(2,1)} %collective-permute-done.refs_10_), channel_id=1, source_target_pairs={{0,8},{8,0},{16,24},{24,16},{1,9},{9,1},{17,25},{25,17},{2,10},{10... | collective-permute-start | bytes 1572872 | tf_op jit(solution)/shard_map/ppermute | solution.py:29
  92.4 4.6 %collective-permute-done.29.refs_9_ = bf16[64,2048]{1,0:T(8,128)(2,1)S(1)} collective-permute-done((bf16[64,2048]{1,0:T(8,128)(2,1)S(1)}, bf16[64,2048]{1,0:T(8,128)(2,1)S(1)}, u32[]{:S(2)}, u32[]{:S(2)}) %collective-permute-start.29) | collective-permute-done | bytes 262176 | tf_op jit(solution)/shard_map/ppermute | solution.py:29
  110.0 3.1 %collective-permute-done.32.refs_13_ = bf16[64,2048]{1,0:T(8,128)(2,1)} collective-permute-done((bf16[64,2048]{1,0:T(8,128)(2,1)S(1)}, bf16[64,2048]{1,0:T(8,128)(2,1)}, u32[]{:S(2)}, u32[]{:S(2)}) %collective-permute-start.32) | collective-permute-done | bytes 262176 | tf_op jit(solution)/shard_map/ppermute | solution.py:29
  114.8 10.5 %collective-permute-done.2.refs_3_ = bf16[128,2048]{1,0:T(8,128)(2,1)} collective-permute-done((bf16[128,2048]{1,0:T(8,128)(2,1)S(1)}, bf16[128,2048]{1,0:T(8,128)(2,1)}, u32[]{:S(2)}, u32[]{:S(2)}) %collective-permute-start.2) | collective-permute-done | bytes 524320 | tf_op jit(solution)/shard_map/ppermute | solution.py:29
  152.4 3.3 %collective-permute-start.59 = (bf16[512,256]{1,0:T(8,128)(2,1)S(1)}, bf16[512,256]{1,0:T(8,128)(2,1)S(1)}, u32[]{:S(2)}, u32[]{:S(2)}) collective-permute-start(bf16[512,256]{1,0:T(8,128)(2,1)S(1)} %get-tuple-element.45), channel_id=1, source_target_pairs={{0,8},{8,0},{16,24},{24,16},{1,9},{9,1},{17,25},{25,17},{2,10},{10... | collective-permute-start | bytes 786440 | tf_op jit(solution)/shard_map/ppermute | solution.py:29
  160.3 11.4 %collective-permute-done.48 = bf16[2,2,64,1024]{3,2,0,1:T(8,128)(2,1)S(1)} collective-permute-done((bf16[2,2,64,1024]{3,2,0,1:T(8,128)(2,1)S(1)}, bf16[2,2,64,1024]{3,2,0,1:T(8,128)(2,1)S(1)}, u32[]{:S(2)}, u32[]{:S(2)}) %collective-permute-start.48) | collective-permute-done | bytes 524320 | tf_op jit(solution)/shard_map/ppermute | solution.py:29
  173.7 2.1 collective-permute-start.51
  176.5 4.7 %collective-permute-done.49 = bf16[2,64,1024]{2,1,0:T(8,128)(2,1)S(1)} collective-permute-done((bf16[2,64,1024]{2,1,0:T(8,128)(2,1)S(1)}, bf16[2,64,1024]{2,1,0:T(8,128)(2,1)S(1)}, u32[]{:S(2)}, u32[]{:S(2)}) %collective-permute-start.49) | collective-permute-done | bytes 262176 | tf_op jit(solution)/shard_map/ppermute | solution.py:29
  181.9 8.8 %collective-permute-done.20 = bf16[2,2,64,1024]{3,2,0,1:T(8,128)(2,1)S(1)} collective-permute-done((bf16[2,2,64,1024]{3,2,0,1:T(8,128)(2,1)S(1)}, bf16[2,2,64,1024]{3,2,0,1:T(8,128)(2,1)S(1)}, u32[]{:S(2)}, u32[]{:S(2)}) %collective-permute-start.20) | collective-permute-done | bytes 524320 | tf_op jit(solution)/shard_map/ppermute | solution.py:29
  192.6 2.6 %collective-permute-start.19 = (bf16[2,64,1024]{2,1,0:T(8,128)(2,1)S(1)}, bf16[2,64,1024]{2,1,0:T(8,128)(2,1)S(1)}, u32[]{:S(2)}, u32[]{:S(2)}) collective-permute-start(bf16[2,64,1024]{2,1,0:T(8,128)(2,1)S(1)} %slice_bitcast_fusion.6), channel_id=1, source_target_pairs={{0,4},{2,6},{4,0},{6,2},{1,5},{3,7},{5,1},{7,3},{8,12},{10,14},{12... | collective-permute-start | bytes 786440 | tf_op jit(solution)/shard_map/ppermute | solution.py:29
  199.6 5.4 %collective-permute-done.53 = bf16[64,2048]{1,0:T(8,128)(2,1)S(1)} collective-permute-done((bf16[64,2048]{1,0:T(8,128)(2,1)S(1)}, bf16[64,2048]{1,0:T(8,128)(2,1)S(1)}, u32[]{:S(2)}, u32[]{:S(2)}) %collective-permute-start.53) | collective-permute-done | bytes 262176 | tf_op jit(solution)/shard_map/ppermute | solution.py:29
  208.3 9.4 %collective-permute-done.52 = bf16[64,2048]{1,0:T(8,128)(2,1)S(1)} collective-permute-done((bf16[64,2048]{1,0:T(8,128)(2,1)S(1)}, bf16[64,2048]{1,0:T(8,128)(2,1)S(1)}, u32[]{:S(2)}, u32[]{:S(2)}) %collective-permute-start.52) | collective-permute-done | bytes 262176 | tf_op jit(solution)/shard_map/ppermute | solution.py:29
  222.0 19.0 %collective-permute-done.62 = bf16[256,512]{1,0:T(8,128)(2,1)S(1)} collective-permute-done((bf16[256,512]{1,0:T(8,128)(2,1)S(1)}, bf16[256,512]{1,0:T(8,128)(2,1)S(1)}, u32[]{:S(2)}, u32[]{:S(2)}) %collective-permute-start.62) | collective-permute-done | bytes 262176 | tf_op jit(solution)/shard_map/ppermute | solution.py:29
  242.7 5.6 %collective-permute-done.57 = bf16[64,2048]{1,0:T(8,128)(2,1)S(1)} collective-permute-done((bf16[64,2048]{1,0:T(8,128)(2,1)S(1)}, bf16[64,2048]{1,0:T(8,128)(2,1)S(1)}, u32[]{:S(2)}, u32[]{:S(2)}) %collective-permute-start.57) | collective-permute-done | bytes 262176 | tf_op jit(solution)/shard_map/ppermute | solution.py:29
  (273 shorter events, 96.8 us)
Async XLA Ops:
  5.8 21.6 %collective-permute-start.12 = (bf16[512,256]{1,0:T(8,128)(2,1)}, bf16[512,256]{1,0:T(8,128)(2,1)S(1)}, u32[]{:S(2)}, u32[]{:S(2)}) collective-permute-start(bf16[512,256]{1,0:T(8,128)(2,1)} %get-tuple-element.59), channel_id=1, source_target_pairs={{0,16},{8,24},{16,0},{24,8},{1,17},{9,25},{17,1},{25,9},{2,18},{10... | collective-permute-start | bytes 786440 | tf_op jit(solution)/shard_map/ppermute | solution.py:29
  8.4 19.7 %collective-permute-start.13 = (bf16[512,256]{1,0:T(8,128)(2,1)}, bf16[512,256]{1,0:T(8,128)(2,1)S(1)}, u32[]{:S(2)}, u32[]{:S(2)}) collective-permute-start(bf16[512,256]{1,0:T(8,128)(2,1)} %get-tuple-element.58), channel_id=1, source_target_pairs={{0,24},{8,16},{16,8},{24,0},{1,25},{9,17},{17,9},{25,1},{2,26},{10... | collective-permute-start | bytes 786440 | tf_op jit(solution)/shard_map/ppermute | solution.py:29
  9.4 25.9 %collective-permute-start.22 = (bf16[64,2048]{1,0:T(8,128)(2,1)S(1)}, bf16[64,2048]{1,0:T(8,128)(2,1)S(1)}, u32[]{:S(2)}, u32[]{:S(2)}) collective-permute-start(bf16[64,2048]{1,0:T(8,128)(2,1)S(1)} %constant_dynamic-slice_fusion.15), channel_id=1, source_target_pairs={{0,8},{8,0},{16,24},{24,16},{1,9},{9,1},{17,25},{25,17},{2,10},{10... | collective-permute-start | bytes 786440 | tf_op jit(solution)/shard_map/ppermute | solution.py:29
  11.3 35.6 %collective-permute-start.26 = (bf16[64,2048]{1,0:T(8,128)(2,1)S(1)}, bf16[64,2048]{1,0:T(8,128)(2,1)}, u32[]{:S(2)}, u32[]{:S(2)}) collective-permute-start(bf16[64,2048]{1,0:T(8,128)(2,1)S(1)} %constant_dynamic-slice_fusion.14), channel_id=1, source_target_pairs={{0,8},{8,0},{16,24},{24,16},{1,9},{9,1},{17,25},{25,17},{2,10},{10... | collective-permute-start | bytes 786440 | tf_op jit(solution)/shard_map/ppermute | solution.py:29
  18.8 32.8 %collective-permute-start.14 = (bf16[256,512]{1,0:T(8,128)(2,1)}, bf16[256,512]{1,0:T(8,128)(2,1)S(1)}, u32[]{:S(2)}, u32[]{:S(2)}) collective-permute-start(bf16[256,512]{1,0:T(8,128)(2,1)} %get-tuple-element.57), channel_id=1, source_target_pairs={{0,8},{8,0},{16,24},{24,16},{1,9},{9,1},{17,25},{25,17},{2,10},{10... | collective-permute-start | bytes 786440 | tf_op jit(solution)/shard_map/ppermute | solution.py:29
  28.1 49.2 %collective-permute-start = (bf16[128,2048]{1,0:T(8,128)(2,1)}, bf16[128,2048]{1,0:T(8,128)(2,1)}, u32[]{:S(2)}, u32[]{:S(2)}) collective-permute-start(bf16[128,2048]{1,0:T(8,128)(2,1)} %pad_maximum_fusion), channel_id=1, source_target_pairs={{0,16},{8,24},{16,0},{24,8},{1,17},{9,25},{17,1},{25,9},{2,18},{10... | collective-permute-start | bytes 1572872 | tf_op jit(solution)/shard_map/ppermute | solution.py:29
  28.8 43.6 %collective-permute-start.15 = (bf16[256,512]{1,0:T(8,128)(2,1)}, bf16[256,512]{1,0:T(8,128)(2,1)S(1)}, u32[]{:S(2)}, u32[]{:S(2)}) collective-permute-start(bf16[256,512]{1,0:T(8,128)(2,1)} %get-tuple-element.56), channel_id=1, source_target_pairs={{0,16},{8,24},{16,0},{24,8},{1,17},{9,25},{17,1},{25,9},{2,18},{10... | collective-permute-start | bytes 786440 | tf_op jit(solution)/shard_map/ppermute | solution.py:29
  35.3 39.3 %collective-permute-start.16 = (bf16[256,512]{1,0:T(8,128)(2,1)}, bf16[256,512]{1,0:T(8,128)(2,1)S(1)}, u32[]{:S(2)}, u32[]{:S(2)}) collective-permute-start(bf16[256,512]{1,0:T(8,128)(2,1)} %get-tuple-element.55), channel_id=1, source_target_pairs={{0,24},{8,16},{16,8},{24,0},{1,25},{9,17},{17,9},{25,1},{2,26},{10... | collective-permute-start | bytes 786440 | tf_op jit(solution)/shard_map/ppermute | solution.py:29
  46.9 29.9 %collective-permute-start.23 = (bf16[64,2048]{1,0:T(8,128)(2,1)S(1)}, bf16[64,2048]{1,0:T(8,128)(2,1)S(1)}, u32[]{:S(2)}, u32[]{:S(2)}) collective-permute-start(bf16[64,2048]{1,0:T(8,128)(2,1)S(1)} %collective-permute-done.22.refs_2_), channel_id=1, source_target_pairs={{0,2},{2,0},{4,6},{6,4},{1,3},{3,1},{5,7},{7,5},{8,10},{10,8},{12,... | collective-permute-start | bytes 786440 | tf_op jit(solution)/shard_map/ppermute | solution.py:29
  52.2 24.6 %collective-permute-start.24 = (bf16[64,2048]{1,0:T(8,128)(2,1)S(1)}, bf16[64,2048]{1,0:T(8,128)(2,1)S(1)}, u32[]{:S(2)}, u32[]{:S(2)}) collective-permute-start(bf16[64,2048]{1,0:T(8,128)(2,1)S(1)} %collective-permute-done.22.refs_2_), channel_id=1, source_target_pairs={{0,4},{2,6},{4,0},{6,2},{1,5},{3,7},{5,1},{7,3},{8,12},{10,14},{12... | collective-permute-start | bytes 786440 | tf_op jit(solution)/shard_map/ppermute | solution.py:29
  77.3 22.4 %collective-permute-start.30 = (bf16[128,2048]{1,0:T(8,128)(2,1)}, bf16[128,2048]{1,0:T(8,128)(2,1)S(1)}, u32[]{:S(2)}, u32[]{:S(2)}) collective-permute-start(bf16[128,2048]{1,0:T(8,128)(2,1)} %collective-permute-done.refs_10_), channel_id=1, source_target_pairs={{0,2},{2,0},{4,6},{6,4},{1,3},{3,1},{5,7},{7,5},{8,10},{10,8},{12,... | collective-permute-start | bytes 1572872 | tf_op jit(solution)/shard_map/ppermute | solution.py:29
  107.0 18.3 %collective-permute-start.2 = (bf16[128,2048]{1,0:T(8,128)(2,1)S(1)}, bf16[128,2048]{1,0:T(8,128)(2,1)}, u32[]{:S(2)}, u32[]{:S(2)}) collective-permute-start(bf16[128,2048]{1,0:T(8,128)(2,1)S(1)} %collective-permute-done.1.refs_2_), channel_id=1, source_target_pairs={{0,2},{2,0},{4,6},{6,4},{1,3},{3,1},{5,7},{7,5},{8,10},{10,8},{12,... | collective-permute-start | bytes 1572872 | tf_op jit(solution)/shard_map/ppermute | solution.py:29
  110.0 22.2 %collective-permute-start.42 = (bf16[128,2048]{1,0:T(8,128)(2,1)}, bf16[128,2048]{1,0:T(8,128)(2,1)}, u32[]{:S(2)}, u32[]{:S(2)}) collective-permute-start(bf16[128,2048]{1,0:T(8,128)(2,1)} %collective-permute-done.refs_10_), channel_id=1, source_target_pairs={{0,1},{1,0},{2,3},{3,2},{4,5},{5,4},{6,7},{7,6},{8,9},{9,8},{10,11... | collective-permute-start | bytes 1572872 | tf_op jit(solution)/shard_map/ppermute | solution.py:29
  113.1 19.2 %collective-permute-start.43 = (bf16[128,2048]{1,0:T(8,128)(2,1)S(1)}, bf16[128,2048]{1,0:T(8,128)(2,1)}, u32[]{:S(2)}, u32[]{:S(2)}) collective-permute-start(bf16[128,2048]{1,0:T(8,128)(2,1)S(1)} %collective-permute-done.30.refs_11_), channel_id=1, source_target_pairs={{0,1},{1,0},{2,3},{3,2},{4,5},{5,4},{6,7},{7,6},{8,9},{9,8},{10,11... | collective-permute-start | bytes 1572872 | tf_op jit(solution)/shard_map/ppermute | solution.py:29
  114.8 18.6 %collective-permute-start.44 = (bf16[128,2048]{1,0:T(8,128)(2,1)S(1)}, bf16[128,2048]{1,0:T(8,128)(2,1)}, u32[]{:S(2)}, u32[]{:S(2)}) collective-permute-start(bf16[128,2048]{1,0:T(8,128)(2,1)S(1)} %collective-permute-done.31.refs_12_), channel_id=1, source_target_pairs={{0,1},{1,0},{2,3},{3,2},{4,5},{5,4},{6,7},{7,6},{8,9},{9,8},{10,11... | collective-permute-start | bytes 1572872 | tf_op jit(solution)/shard_map/ppermute | solution.py:29
  149.1 23.4 %collective-permute-start.17 = (bf16[512,2048]{1,0:T(8,128)(2,1)S(1)}, bf16[512,2048]{1,0:T(8,128)(2,1)S(1)}, u32[]{:S(2)}, u32[]{:S(2)}) collective-permute-start(bf16[512,2048]{1,0:T(8,128)(2,1)S(1)} %convolution_convert_fusion.1), channel_id=1, source_target_pairs={{0,1},{1,0},{2,3},{3,2},{4,5},{5,4},{6,7},{7,6},{8,9},{9,8},{10,11... | collective-permute-start | bytes 6291464 | tf_op jit(solution)/shard_map/ppermute | solution.py:29
  152.4 67.5 %collective-permute-start.59 = (bf16[512,256]{1,0:T(8,128)(2,1)S(1)}, bf16[512,256]{1,0:T(8,128)(2,1)S(1)}, u32[]{:S(2)}, u32[]{:S(2)}) collective-permute-start(bf16[512,256]{1,0:T(8,128)(2,1)S(1)} %get-tuple-element.45), channel_id=1, source_target_pairs={{0,8},{8,0},{16,24},{24,16},{1,9},{9,1},{17,25},{25,17},{2,10},{10... | collective-permute-start | bytes 786440 | tf_op jit(solution)/shard_map/ppermute | solution.py:29
  155.6 66.3 %collective-permute-start.60 = (bf16[512,256]{1,0:T(8,128)(2,1)S(1)}, bf16[512,256]{1,0:T(8,128)(2,1)S(1)}, u32[]{:S(2)}, u32[]{:S(2)}) collective-permute-start(bf16[512,256]{1,0:T(8,128)(2,1)S(1)} %get-tuple-element.44), channel_id=1, source_target_pairs={{0,16},{8,24},{16,0},{24,8},{1,17},{9,25},{17,1},{25,9},{2,18},{10... | collective-permute-start | bytes 786440 | tf_op jit(solution)/shard_map/ppermute | solution.py:29
  197.8 20.0 %collective-permute-start.52 = (bf16[64,2048]{1,0:T(8,128)(2,1)S(1)}, bf16[64,2048]{1,0:T(8,128)(2,1)S(1)}, u32[]{:S(2)}, u32[]{:S(2)}) collective-permute-start(bf16[64,2048]{1,0:T(8,128)(2,1)S(1)} %get-tuple-element.61), channel_id=1, source_target_pairs={{0,8},{8,0},{16,24},{24,16},{1,9},{9,1},{17,25},{25,17},{2,10},{10... | collective-permute-start | bytes 786440 | tf_op jit(solution)/shard_map/ppermute | solution.py:29
  217.8 23.3 %collective-permute-start.62 = (bf16[256,512]{1,0:T(8,128)(2,1)S(1)}, bf16[256,512]{1,0:T(8,128)(2,1)S(1)}, u32[]{:S(2)}, u32[]{:S(2)}) collective-permute-start(bf16[256,512]{1,0:T(8,128)(2,1)S(1)} %get-tuple-element.48), channel_id=1, source_target_pairs={{0,16},{8,24},{16,0},{24,8},{1,17},{9,25},{17,1},{25,9},{2,18},{10... | collective-permute-start | bytes 786440 | tf_op jit(solution)/shard_map/ppermute | solution.py:29
  217.8 24.1 %collective-permute-start.63 = (bf16[256,512]{1,0:T(8,128)(2,1)S(1)}, bf16[256,512]{1,0:T(8,128)(2,1)S(1)}, u32[]{:S(2)}, u32[]{:S(2)}) collective-permute-start(bf16[256,512]{1,0:T(8,128)(2,1)S(1)} %get-tuple-element.47), channel_id=1, source_target_pairs={{0,24},{8,16},{16,8},{24,0},{1,25},{9,17},{17,9},{25,1},{2,26},{10... | collective-permute-start | bytes 786440 | tf_op jit(solution)/shard_map/ppermute | solution.py:29
  219.9 28.7 %collective-permute-start.64 = (bf16[512,256]{1,0:T(8,128)(2,1)S(1)}, bf16[512,256]{1,0:T(8,128)(2,1)S(1)}, u32[]{:S(2)}, u32[]{:S(2)}) collective-permute-start(bf16[512,256]{1,0:T(8,128)(2,1)S(1)} %get-tuple-element.43), channel_id=1, source_target_pairs={{0,24},{8,16},{16,8},{24,0},{1,25},{9,17},{17,9},{25,1},{2,26},{10... | collective-permute-start | bytes 786440 | tf_op jit(solution)/shard_map/ppermute | solution.py:29
  221.9 20.7 %collective-permute-start.55 = (bf16[64,2048]{1,0:T(8,128)(2,1)S(1)}, bf16[64,2048]{1,0:T(8,128)(2,1)S(1)}, u32[]{:S(2)}, u32[]{:S(2)}) collective-permute-start(bf16[64,2048]{1,0:T(8,128)(2,1)S(1)} %get-tuple-element.38), channel_id=1, source_target_pairs={{0,2},{2,0},{4,6},{6,4},{1,3},{3,1},{5,7},{7,5},{8,10},{10,8},{12,... | collective-permute-start | bytes 786440 | tf_op jit(solution)/shard_map/ppermute | solution.py:29
  221.9 20.7 %collective-permute-start.56 = (bf16[64,2048]{1,0:T(8,128)(2,1)S(1)}, bf16[64,2048]{1,0:T(8,128)(2,1)S(1)}, u32[]{:S(2)}, u32[]{:S(2)}) collective-permute-start(bf16[64,2048]{1,0:T(8,128)(2,1)S(1)} %get-tuple-element.38), channel_id=1, source_target_pairs={{0,4},{2,6},{4,0},{6,2},{1,5},{3,7},{5,1},{7,3},{8,12},{10,14},{12... | collective-permute-start | bytes 786440 | tf_op jit(solution)/shard_map/ppermute | solution.py:29
  (90 other events, 638.8 us)
